TPU v7x, 512 devices: a whole 4x4x16 slice. The times are simulated.
512 devices in a mesh: ep: 32 (over z, core), tp: 16 (over y, x).
Axes of the slice: x: 4, y: 4, z: 16, core: 2. Of those that a mesh axis runs over, the one named last changes fastest.
Arguments:
- mixer_input: bfloat16 [8192, 1024], P('ep', 'tp'), may hold values from -6 to 6
- log_step: float32 [64], P('tp'), may hold values from -12.8 to -2.7
- decay_shift: float32 [8192, 64], P('ep', 'tp'), may hold values from -2 to 0
- input_map: bfloat16 [2, 64, 64, 16], P(None, 'tp'), may hold values from -143.10835 to 143.10835
- readout: float32 [2, 64, 16, 64], P(None, 'tp'), may hold values from -0.5 to 0.5
- mixer_weight: bfloat16 [1024, 2048], P(None, 'tp'), may hold values from -0.1875 to 0.1875
- expert_input: bfloat16 [4096, 2048], P('ep'), may hold values from -6 to 6
- norm_gain: float32 [2048], replicated, may hold values from 0.1 to 1.9
- routes: int32 [4096, 2], P('ep'), may hold values from 0 to 31, all different within a row; in each aligned block of 128 rows (0 to 127, 128 to 255, ...) at most 16 rows name the same one
- route_weight: float32 [4096, 2], P('ep'), may hold values from 0.1 to 2.5
- expert_switch_matrix: bfloat16 [32, 2048, 4096], P('ep', None, 'tp'), may hold values from -0.125 to 0.125
- up_weight: bfloat16 [32, 2048, 4096], P('ep', None, 'tp'), may hold values from -0.125 to 0.125
- down_weight: bfloat16 [32, 4096, 2048], P('ep', None, 'tp'), may hold values from -0.09375 to 0.09375
- shared_gate: bfloat16 [2048, 1024], P(None, 'tp'), may hold values from -0.125 to 0.125
- shared_up: bfloat16 [2048, 1024], P(None, 'tp'), may hold values from -0.125 to 0.125
- shared_down: bfloat16 [1024, 2048], P(None, 'tp'), may hold values from -0.1875 to 0.1875
Outputs:
- mixer_out: bfloat16 [8192, 2048], P('ep', 'tp')
- experts_out: bfloat16 [4096, 2048], P('ep', 'tp')
Inputs may be any that keep to these rules, and one draw needn't show every extreme that they name: `routes`: each row names 2 different experts. In each aligned block of 128 rows (the rows of one index of ep) no expert is named by more than 16 rows, and in some block one expert is named by exactly 16 rows.
All inputs are finite; a program needn't handle non-finite values.
Results may differ from a plain program's by a relative error of at most 0.0069.
Values may be sent and summed in bfloat16 or wider, within the bound.
A program may use at most 64 MiB of HBM per device.

v0:
```python
import jax
import jax.numpy as jnp
from jax import lax
from jax.sharding import Mesh
from jax.sharding import PartitionSpec as P

TP = ("tp_0", "tp_1")


def sent_to_all(shard, axis):
    copies = jnp.broadcast_to(shard, (lax.axis_size(axis), *shard.shape))
    return lax.all_to_all(copies, axis, split_axis=0, concat_axis=0, tiled=True)


def gathered_once(shard, axis):
    leaves = jax.tree.leaves(shard)
    turns = sorted(range(len(leaves)), key=lambda k: -leaves[k].size)
    width = (1, *leaves[turns[0]].shape)[-1]
    lines = [
        jnp.pad(leaves[k].reshape(-1), (0, -leaves[k].size % width)).reshape(-1, width)
        for k in turns
    ]
    both, at, found = (sent_to_all(jnp.concatenate(lines), axis), 0, {})
    for k, line in zip(turns, lines):
        share = both[:, at : at + len(line)].reshape(len(both), -1)
        found[k] = share[:, : leaves[k].size].reshape(-1, *leaves[k].shape)
        at += len(line)
    numbers = iter(range(len(leaves)))
    return jax.tree.map(lambda _: found[next(numbers)], shard)


def joined_by_halves(pieces, combine):
    while len(jax.tree.leaves(pieces)[0]) > 1:
        pieces = jax.vmap(combine)(
            *(jax.tree.map(lambda part: part[side::2], pieces) for side in (0, 1))
        )
    return jax.tree.map(lambda part: part[0], pieces)


def carried_in(shard, axis, combine, identity):
    count, index = (lax.axis_size(axis), lax.axis_index(axis))
    passed = jnp.arange(count) < index

    def kept(part, zero, own):
        part = jnp.where(
            passed.reshape(-1, *(1 for _ in own.shape)), part, jnp.asarray(zero, own.dtype)
        )
        return part

    pieces = gathered_once(shard, axis)
    return joined_by_halves(jax.tree.map(kept, pieces, identity, shard), combine)


def joined_along(blocks, dim):
    blocks = jnp.moveaxis(blocks, 0, dim)
    shape = blocks.shape
    return blocks.reshape(*shape[:dim], shape[dim] * shape[dim + 1], *shape[dim + 2 :])


def gathered_copies(shard, axis, dim):
    return joined_along(sent_to_all(shard, axis), dim)


def whole_of(shard, axes, dim):
    for axis in reversed(axes):
        shard = lax.all_gather(shard, axis, axis=dim, tiled=True)
    return shard


def combine_parts(earlier, later):
    early_real, early_imaginary, early_shift_real, early_shift_imaginary = earlier
    late_real, late_imaginary, late_shift_real, late_shift_imaginary = later
    joint_real = late_real * early_real - late_imaginary * early_imaginary
    joint_imaginary = late_real * early_imaginary + late_imaginary * early_real
    shift_real = (
        late_real * early_shift_real - late_imaginary * early_shift_imaginary + late_shift_real
    )
    shift_imaginary = (
        late_real * early_shift_imaginary + late_imaginary * early_shift_real + late_shift_imaginary
    )
    return (joint_real, joint_imaginary, shift_real, shift_imaginary)


def factors(log_step, states):
    step_rate = jnp.exp(log_step)
    frequency = jnp.pi * jnp.arange(states, dtype=jnp.float32)
    angle = step_rate[:, None] * frequency[None, :]
    turn_cosine = jnp.cos(angle)
    turn_sine = jnp.sin(angle)
    base = jnp.exp(-0.5 * step_rate)[:, None]
    base_real = base * turn_cosine
    starting_quadrature = base * turn_sine
    inverse = 1.0 / (0.25 + frequency * frequency)[None, :]
    lowered = base_real - 1.0
    inject_real = (-0.5 * lowered + starting_quadrature * frequency[None, :]) * inverse
    inject_imaginary = (-0.5 * starting_quadrature - lowered * frequency[None, :]) * inverse
    return (step_rate, turn_cosine, turn_sine, inject_real, inject_imaginary)


def shards(
    mixer_input,
    log_step,
    decay_shift,
    input_map,
    readout,
    mixer_weight,
    expert_input,
    norm_gain,
    routes,
    route_weight,
    expert_switch_matrix,
    up_weight,
    down_weight,
    shared_gate,
    shared_up,
    shared_down,
):
    highest = lax.Precision.HIGHEST
    row_count = mixer_input.shape[0]
    groups = log_step.shape[0]
    states = input_map.shape[2]
    width = input_map.shape[3]
    merged = groups * states
    channels = groups * width
    step_rate, turn_cosine, turn_sine, inject_real, inject_imaginary = factors(log_step, states)
    magnitude = jnp.exp(-0.5 * step_rate[None, :] + decay_shift)[:, :, None]
    decay_real = (magnitude * turn_cosine[None]).reshape(row_count, merged)
    decay_imaginary = (magnitude * turn_sine[None]).reshape(row_count, merged)
    identity = jnp.eye(groups, dtype=jnp.float32)
    spread_in = jnp.einsum("cgph,gk->hcgkp", input_map.astype(jnp.float32), identity)
    spread_in = spread_in.reshape(width, 2, groups, groups * states)
    spread_in = (
        jnp.transpose(spread_in, (2, 0, 1, 3)).reshape(channels, 2 * merged).astype(jnp.bfloat16)
    )
    drive = jnp.dot(mixer_input, spread_in, preferred_element_type=jnp.float32)
    drive_real = drive[:, :merged]
    drive_imaginary = drive[:, merged:]
    flat_inject_real = inject_real.reshape(1, merged)
    flat_inject_imaginary = inject_imaginary.reshape(1, merged)
    push_real = flat_inject_real * drive_real - flat_inject_imaginary * drive_imaginary
    push_imaginary = flat_inject_real * drive_imaginary + flat_inject_imaginary * drive_real
    total_real, total_imaginary, local_real, local_imaginary = lax.associative_scan(
        combine_parts, (decay_real, decay_imaginary, push_real, push_imaginary), axis=0
    )
    summary = (total_real[-1], total_imaginary[-1], local_real[-1], local_imaginary[-1])
    neutral = (
        jnp.ones_like(summary[0]),
        jnp.zeros_like(summary[0]),
        jnp.zeros_like(summary[0]),
        jnp.zeros_like(summary[0]),
    )
    incoming = carried_in(summary, "ep", combine_parts, neutral)
    carry_real = incoming[2]
    carry_imaginary = incoming[3]
    state_real = (
        local_real + total_real * carry_real[None] - total_imaginary * carry_imaginary[None]
    )
    state_imaginary = (
        local_imaginary + total_real * carry_imaginary[None] + total_imaginary * carry_real[None]
    )
    signed = jnp.stack([readout[0], -readout[1]], axis=0)
    spread_out = jnp.einsum("cghp,gk->cgpkh", signed, identity, precision=highest).reshape(
        2 * merged, channels
    )
    both_states = jnp.concatenate([state_real, state_imaginary], axis=1)
    mixed = jnp.dot(both_states, spread_out, precision=highest)
    activated = jax.nn.gelu(mixed).astype(jnp.bfloat16)
    mixer_out = jnp.dot(
        gathered_copies(activated, TP, 1), mixer_weight, preferred_element_type=jnp.float32
    ).astype(jnp.bfloat16)
    token_count = expert_input.shape[0]
    top_count = routes.shape[1]
    experts = lax.axis_size("ep")
    capacity = 2 * token_count * top_count // experts
    values = expert_input.astype(jnp.float32)
    normed = (
        values * lax.rsqrt(jnp.mean(values * values, axis=-1, keepdims=True) + 1e-06) * norm_gain
    ).astype(jnp.bfloat16)
    flat_routes = routes.reshape(-1)
    onehot = (flat_routes[:, None] == jnp.arange(experts, dtype=jnp.int32)[None, :]).astype(
        jnp.int32
    )
    before = jnp.sum((jnp.cumsum(onehot, axis=0) - onehot) * onehot, axis=1)
    slot = flat_routes * capacity + before
    owner = jnp.arange(flat_routes.shape[0], dtype=jnp.int32) // top_count
    slot_token = jnp.full((experts * capacity,), token_count, jnp.int32).at[slot].set(owner)
    slice_width = down_weight.shape[2]
    received_rows = experts * capacity
    own_columns = lax.dynamic_slice_in_dim(normed, lax.axis_index(TP) * slice_width, slice_width, 1)
    padded = jnp.concatenate([own_columns, jnp.zeros((1, slice_width), jnp.bfloat16)], axis=0)
    outgoing = padded[slot_token].reshape(experts, capacity, slice_width)
    arrived = lax.all_to_all(outgoing, "ep", split_axis=0, concat_axis=0, tiled=True).reshape(
        received_rows, slice_width
    )
    piece = whole_of(arrived, TP, 1)
    gate_rows = expert_switch_matrix[0]
    up_rows = up_weight[0]
    gate_sum = jnp.dot(piece, gate_rows, preferred_element_type=jnp.float32)
    up_sum = jnp.dot(piece, up_rows, preferred_element_type=jnp.float32)
    expert_hidden = (jax.nn.silu(gate_sum) * up_sum).astype(jnp.bfloat16)
    shared_hidden = (
        jax.nn.silu(jnp.dot(normed, shared_gate, preferred_element_type=jnp.float32))
        * jnp.dot(normed, shared_up, preferred_element_type=jnp.float32)
    ).astype(jnp.bfloat16)
    rows_here = down_weight[0]
    routed_output = jnp.dot(
        lax.all_gather(expert_hidden, TP, axis=1, tiled=True),
        rows_here,
        preferred_element_type=jnp.float32,
    )
    rows_here = shared_down
    common_contribution = jnp.dot(
        gathered_copies(shared_hidden, TP, 1), rows_here, preferred_element_type=jnp.float32
    )
    returned = lax.all_to_all(
        routed_output.astype(jnp.bfloat16).reshape(experts, capacity, slice_width),
        "ep",
        split_axis=0,
        concat_axis=0,
        tiled=True,
    ).reshape(received_rows, slice_width)
    picked = returned[slot].reshape(token_count, top_count, slice_width).astype(jnp.float32)
    experts_out = (common_contribution + jnp.sum(route_weight[:, :, None] * picked, axis=1)).astype(
        jnp.bfloat16
    )
    return (mixer_out, experts_out)


def solution(mesh):
    torus = Mesh(mesh.devices.reshape(mesh.shape["ep"], 4, 4), ("ep", "tp_0", "tp_1"))
    placed = (
        P("ep", TP),
        P(TP),
        P("ep", TP),
        P(None, TP, None, None),
        P(None, TP, None, None),
        P(None, TP),
        P("ep", None),
        P(),
        P("ep", None),
        P("ep", None),
        P("ep", None, TP),
        P("ep", None, TP),
        P("ep", None, TP),
        P(None, TP),
        P(None, TP),
        P(None, TP),
    )
    return jax.shard_map(
        shards, mesh=torus, in_specs=placed, out_specs=(P("ep", TP), P("ep", TP)), check_vma=False
    )
```

profile of v0, /device:TPU:1, one launch (start us, length us, event | category | flops | bytes accessed | tf_op | source)
XLA Modules:
  0.0 233.4 jit_solution(8538486471405758539)
XLA Ops:
  9.1 1.2 fusion.3
  12.0 1.4 scatter_custom_fusion
  13.5 1.2 fusion.5
  14.8 1.9 gather_fusion
  16.7 16.7 %all-to-all-start.3 = ((bf16[32,16,128]{2,1,0:T(8,128)(2,1)}), bf16[32,16,128]{2,1,0:T(8,128)(2,1)S(1)}, u32[]{:S(2)}, u32[]{:S(2)}) async-start(bf16[32,16,128]{2,1,0:T(8,128)(2,1)} %bitcast.19), calls=%async_computation.3 | async-start | bytes 262144 | tf_op jit(solution)/shard_map/all_to_all | solution.py:192
  39.6 1.0 multiply_subtract_fusion.3
  43.0 6.3 %all-to-all-done.3 = bf16[32,16,128]{2,1,0:T(8,128)(2,1)S(1)} async-done(((bf16[32,16,128]{2,1,0:T(8,128)(2,1)}), bf16[32,16,128]{2,1,0:T(8,128)(2,1)S(1)}, u32[]{:S(2)}, u32[]{:S(2)}) %all-to-all-start.3) | async-done | bytes 131104 | tf_op jit(solution)/shard_map/all_to_all | solution.py:192
  49.3 12.8 %all_gather.9 = bf16[512,512]{1,0:T(8,128)(2,1)} all-gather(bf16[512,128]{1,0:T(8,128)(2,1)S(1)} %bitcast.96), channel_id=1, replica_groups=mesh['ep'=32,'tp_0'=4,'tp_1'=4] {'tp_1'}, dimensions={1}, use_global_device_ids=true | all-gather | bytes 655360 | tf_op jit(solution)/shard_map/all_gather | solution.py:66
  63.0 33.3 %all-gather.3.cloned.1.call-done = bf16[512,2048]{1,0:T(8,128)(2,1)} async-done(((bf16[512,512]{1,0:T(8,128)(2,1)}), bf16[512,2048]{1,0:T(8,128)(2,1)}) %all-gather.3.cloned.1.call-update) | async-done | bytes 2097168 | tf_op jit(solution)/shard_map/all_gather | solution.py:66
  96.3 2.4 %fusion.8 = f32[512,256]{1,0:T(8,128)S(1)} fusion(bf16[512,2048]{1,0:T(8,128)(2,1)} %all-gather.3.cloned.1.call-done, bf16[1,2048,256]{2,1,0:T(8,128)(2,1)S(1)} %copy-done), kind=kOutput, calls=%fused_computation.19 | convolution fusion | flops 536870912 | bytes 3670016 | tf_op jit(solution)/shard_map/dot_general | solution.py:198
  98.8 1.4 fusion
  102.8 1.0 pad.226
  103.8 1.5 pad.260
  106.7 13.2 %all-to-all-start = ((f32[32,4,256]{2,1,0:T(4,128)}), f32[32,4,256]{2,1,0:T(4,128)}, u32[]{:S(2)}, u32[]{:S(2)}) async-start(f32[32,4,256]{2,1,0:T(4,128)} %broadcast_in_dim.60), calls=%async_computation | async-start | bytes 262144 | tf_op jit(solution)/shard_map/all_to_all | solution.py:12
  121.5 1.1 reshape.277
  122.7 13.1 %all-to-all-done = f32[32,4,256]{2,1,0:T(4,128)} async-done(((f32[32,4,256]{2,1,0:T(4,128)}), f32[32,4,256]{2,1,0:T(4,128)}, u32[]{:S(2)}, u32[]{:S(2)}) %all-to-all-start) | async-done | bytes 131104 | tf_op jit(solution)/shard_map/all_to_all | solution.py:12
  135.8 1.4 fusion.44
  137.9 1.4 slice.786
  139.3 1.4 slice.785
  140.6 1.4 slice.789
  142.0 1.4 slice.788
  143.4 1.4 slice.807
  144.7 1.4 slice.804
  146.1 1.4 slice.809
  147.4 1.4 slice.806
  148.8 1.5 multiply_subtract_fusion.8
  150.3 1.3 slice.791
  151.6 1.3 slice.790
  152.9 1.3 slice.793
  154.2 1.3 slice.792
  155.5 1.3 slice.813
  156.8 1.3 slice.810
  159.4 1.4 multiply_subtract_fusion.11
  160.8 1.3 slice.795
  162.1 1.3 slice.794
  163.4 1.3 slice.797
  164.7 1.3 slice.796
  173.6 1.1 multiply_subtract_fusion
  176.2 5.3 %all-to-all-start.1 = ((bf16[16,256,64]{1,2,0:T(8,128)(2,1)}), bf16[16,256,64]{1,2,0:T(8,128)(2,1)S(1)}, u32[]{:S(2)}, u32[]{:S(2)}) async-start(bf16[16,256,64]{1,2,0:T(8,128)(2,1)} %broadcast_in_dim.63), calls=%async_computation.1 | async-start | bytes 1048576 | tf_op jit(solution)/shard_map/all_to_all | solution.py:12
  181.6 4.4 %convolution_convert_fusion = bf16[512,128]{1,0:T(8,128)(2,1)} fusion(bf16[512,4096]{1,0:T(8,128)(2,1)} %all-gather.5.cloned.1.call-done, bf16[1,4096,128]{2,1,0:T(8,128)(2,1)} %param.28), kind=kOutput, calls=%fused_computation.8 | convolution fusion | flops 536936448 | bytes 5373952 | tf_op jit(solution)/shard_map/dot_general | solution.py:206
  186.0 5.5 %all-to-all-done.1 = bf16[16,256,64]{1,2,0:T(8,128)(2,1)S(1)} async-done(((bf16[16,256,64]{1,2,0:T(8,128)(2,1)}), bf16[16,256,64]{1,2,0:T(8,128)(2,1)S(1)}, u32[]{:S(2)}, u32[]{:S(2)}) %all-to-all-start.1) | async-done | bytes 524320 | tf_op jit(solution)/shard_map/all_to_all | solution.py:12
  191.5 6.0 %all-to-all-start.4 = ((bf16[32,16,128]{2,1,0:T(8,128)(2,1)}), bf16[32,16,128]{2,1,0:T(8,128)(2,1)S(1)}, u32[]{:S(2)}, u32[]{:S(2)}) async-start(bf16[32,16,128]{2,1,0:T(8,128)(2,1)} %bitcast.24), calls=%async_computation.4 | async-start | bytes 262144 | tf_op jit(solution)/shard_map/all_to_all | solution.py:215
  198.3 15.4 %all-to-all-done.4 = bf16[32,16,128]{2,1,0:T(8,128)(2,1)S(1)} async-done(((bf16[32,16,128]{2,1,0:T(8,128)(2,1)}), bf16[32,16,128]{2,1,0:T(8,128)(2,1)S(1)}, u32[]{:S(2)}, u32[]{:S(2)}) %all-to-all-start.4) | async-done | bytes 131104 | tf_op jit(solution)/shard_map/all_to_all | solution.py:215
  214.4 3.5 %all-to-all-start.2 = ((bf16[16,128,64]{1,2,0:T(8,128)(2,1)}), bf16[16,128,64]{1,2,0:T(8,128)(2,1)S(1)}, u32[]{:S(2)}, u32[]{:S(2)}) async-start(bf16[16,128,64]{1,2,0:T(8,128)(2,1)} %broadcast_in_dim.64), calls=%async_computation.2 | async-start | bytes 524288 | tf_op jit(solution)/shard_map/all_to_all | solution.py:12
  218.0 1.0 convolution_convert_fusion.1
  219.0 0.9 gather_fusion.1
  220.1 5.6 %all-to-all-done.2 = bf16[16,128,64]{1,2,0:T(8,128)(2,1)S(1)} async-done(((bf16[16,128,64]{1,2,0:T(8,128)(2,1)}), bf16[16,128,64]{1,2,0:T(8,128)(2,1)S(1)}, u32[]{:S(2)}, u32[]{:S(2)}) %all-to-all-start.2) | async-done | bytes 262176 | tf_op jit(solution)/shard_map/all_to_all | solution.py:12
  225.7 0.9 fusion.1
  (364 shorter events, 30.1 us)
Async XLA Ops:
  7.2 89.1 %copy-start = (bf16[1,2048,256]{2,1,0:T(8,128)(2,1)S(1)}, bf16[1,2048,256]{2,1,0:T(8,128)(2,1)}, u32[]{:S(2)}) copy-start(bf16[1,2048,256]{2,1,0:T(8,128)(2,1)} %param.26) | copy-start | bytes 3145732
  7.2 26.4 %copy-start.14 = (f32[4]{0:T(128)S(1)}, f32[4]{0:T(128)}, u32[]{:S(2)}) copy-start(f32[4]{0:T(128)} %param.17) | copy-start | bytes 52
  7.2 27.2 %copy-start.12 = (f32[256,4]{0,1:T(4,128)S(1)}, f32[256,4]{0,1:T(4,128)}, u32[]{:S(2)}) copy-start(f32[256,4]{0,1:T(4,128)} %param.18) | copy-start | bytes 12292
  7.2 27.3 %copy-start.5 = (bf16[2,4,64,16]{2,3,1,0:T(8,128)(2,1)S(1)}, bf16[2,4,64,16]{2,3,1,0:T(8,128)(2,1)}, u32[]{:S(2)}) copy-start(bf16[2,4,64,16]{2,3,1,0:T(8,128)(2,1)} %param.19) | copy-start | bytes 49156
  11.5 0.5 copy-start.10
  13.5 21.5 %copy-start.6 = (bf16[256,64]{0,1:T(8,128)(2,1)S(1)}, bf16[256,64]{0,1:T(8,128)(2,1)}, u32[]{:S(2)}) copy-start(bf16[256,64]{0,1:T(8,128)(2,1)} %param.16) | copy-start | bytes 98308
  16.7 32.6 %all-to-all-start.3 = ((bf16[32,16,128]{2,1,0:T(8,128)(2,1)}), bf16[32,16,128]{2,1,0:T(8,128)(2,1)S(1)}, u32[]{:S(2)}, u32[]{:S(2)}) async-start(bf16[32,16,128]{2,1,0:T(8,128)(2,1)} %bitcast.19), calls=%async_computation.3 | async-start | bytes 262144 | tf_op jit(solution)/shard_map/all_to_all | solution.py:192
  33.4 62.9 %all-gather.3.cloned.1.call-start = ((), (), s32[]{:S(2)}) async-start(), calls=%async_computation.5 | async-start | bytes 2621440 | tf_op jit(solution)/shard_map/all_gather | solution.py:66
  34.5 1.2 copy-start.7
  40.8 1.7 slice-start
  62.1 119.4 %all-gather.5.cloned.1.call-start = ((), (), s32[]{:S(2)}) async-start(), calls=%async_computation.6 | async-start | bytes 4456448 | tf_op jit(solution)/shard_map/all_gather | solution.py:207
  96.3 2.5 %copy-start.15 = (bf16[512,2048]{1,0:T(8,128)(2,1)S(1)}, bf16[512,2048]{1,0:T(8,128)(2,1)}, u32[]{:S(2)}) copy-start(bf16[512,2048]{1,0:T(8,128)(2,1)} %all-gather.3.cloned.1.call-done) | copy-start | bytes 6291460
  96.3 2.5 %copy-start.16 = (bf16[1,2048,256]{2,1,0:T(8,128)(2,1)S(1)}, bf16[1,2048,256]{2,1,0:T(8,128)(2,1)}, u32[]{:S(2)}) copy-start(bf16[1,2048,256]{2,1,0:T(8,128)(2,1)} %param.27) | copy-start | bytes 3145732
  101.0 1.1 copy-start.9
  102.0 0.7 copy-start.8
  106.7 29.1 %all-to-all-start = ((f32[32,4,256]{2,1,0:T(4,128)}), f32[32,4,256]{2,1,0:T(4,128)}, u32[]{:S(2)}, u32[]{:S(2)}) async-start(f32[32,4,256]{2,1,0:T(4,128)} %broadcast_in_dim.60), calls=%async_computation | async-start | bytes 262144 | tf_op jit(solution)/shard_map/all_to_all | solution.py:12
  176.2 15.3 %all-to-all-start.1 = ((bf16[16,256,64]{1,2,0:T(8,128)(2,1)}), bf16[16,256,64]{1,2,0:T(8,128)(2,1)S(1)}, u32[]{:S(2)}, u32[]{:S(2)}) async-start(bf16[16,256,64]{1,2,0:T(8,128)(2,1)} %broadcast_in_dim.63), calls=%async_computation.1 | async-start | bytes 1048576 | tf_op jit(solution)/shard_map/all_to_all | solution.py:12
  181.5 16.0 %copy-start.11 = (s32[256,1]{0,1:T(1,128)S(1)}, s32[256,1]{0,1:T(1,128)}, u32[]{:S(2)}) copy-start(s32[256,1]{0,1:T(1,128)} %copy-done.10) | copy-start | bytes 3076
  181.5 16.1 %copy-start.13 = (f32[128,2]{0,1:T(2,128)S(1)}, f32[128,2]{0,1:T(2,128)}, u32[]{:S(2)}) copy-start(f32[128,2]{0,1:T(2,128)} %param.25) | copy-start | bytes 3076
  181.5 16.2 %copy-start.1 = (bf16[2048,64]{0,1:T(8,128)(2,1)S(1)}, bf16[2048,64]{0,1:T(8,128)(2,1)}, u32[]{:S(2)}) copy-start(bf16[2048,64]{0,1:T(8,128)(2,1)} %param.29) | copy-start | bytes 786436
  181.5 16.5 %copy-start.2 = (bf16[2048,64]{0,1:T(8,128)(2,1)S(1)}, bf16[2048,64]{0,1:T(8,128)(2,1)}, u32[]{:S(2)}) copy-start(bf16[2048,64]{0,1:T(8,128)(2,1)} %param.30) | copy-start | bytes 786436
  186.0 32.0 %copy-start.3 = (bf16[1024,128]{1,0:T(8,128)(2,1)S(1)}, bf16[1024,128]{1,0:T(8,128)(2,1)}, u32[]{:S(2)}) copy-start(bf16[1024,128]{1,0:T(8,128)(2,1)} %param.21) | copy-start | bytes 786436
  191.5 22.2 %all-to-all-start.4 = ((bf16[32,16,128]{2,1,0:T(8,128)(2,1)}), bf16[32,16,128]{2,1,0:T(8,128)(2,1)S(1)}, u32[]{:S(2)}, u32[]{:S(2)}) async-start(bf16[32,16,128]{2,1,0:T(8,128)(2,1)} %bitcast.24), calls=%async_computation.4 | async-start | bytes 262144 | tf_op jit(solution)/shard_map/all_to_all | solution.py:215
  197.5 28.1 %copy-start.4 = (bf16[1024,128]{1,0:T(8,128)(2,1)S(1)}, bf16[1024,128]{1,0:T(8,128)(2,1)}, u32[]{:S(2)}) copy-start(bf16[1024,128]{1,0:T(8,128)(2,1)} %param.31) | copy-start | bytes 786436
  214.4 11.2 %all-to-all-start.2 = ((bf16[16,128,64]{1,2,0:T(8,128)(2,1)}), bf16[16,128,64]{1,2,0:T(8,128)(2,1)S(1)}, u32[]{:S(2)}, u32[]{:S(2)}) async-start(bf16[16,128,64]{1,2,0:T(8,128)(2,1)} %broadcast_in_dim.64), calls=%async_computation.2 | async-start | bytes 524288 | tf_op jit(solution)/shard_map/all_to_all | solution.py:12
Sparse Core Ops, SparseCore 0:
  62.3 33.9 all-gather.2
  100.3 70.9 all-gather.4
where the time goes:
time: 235 us; the launch traced here: 233 us
  waiting for transfers between devices  79.2 us (34%)
  local copies, waits for them, and re-layouts  52.1 us (22%)
  starting transfers between devices  44.9 us (19%)
  other arithmetic  16.9 us (7%)
  between operations  15.8 us (7%)
  blocking collectives  12.8 us (5%)
  matrix products  11.7 us (5%)
    all_gather x1, waiting for transfers between devices, whole_of(): shard = lax.all_gather(shard, axis, axis=dim, tiled=True)  33.3 us
    slice x32, local copies, waits for them, and re-layouts, joined_by_halves(): part[side::2]  30.6 us
    all_to_all x3, waiting for transfers between devices, sent_to_all(): return lax.all_to_all(copies, axis, split_axis=0, concat_axis=0, tiled=True)  24.2 us
    all_to_all x3, starting transfers between devices, sent_to_all(): return lax.all_to_all(copies, axis, split_axis=0, concat_axis=0, tiled=True)  22 us
    all_to_all x1, starting transfers between devices, shards(): lax.all_to_all(outgoing, 'ep', split_axis=0, concat_axis=0, tiled=True)  16.7 us
    all_to_all x1, waiting for transfers between devices, shards(): lax.all_to_all(routed_output.astype(jnp.bfloat16).reshape(experts, capaci...  15.4 us
    all_gather x1, blocking collectives, whole_of(): shard = lax.all_gather(shard, axis, axis=dim, tiled=True)  12.8 us
    all_to_all x1, waiting for transfers between devices, shards(): lax.all_to_all(outgoing, 'ep', split_axis=0, concat_axis=0, tiled=True)  6.26 us
  transfers between devices with their start and end apart: 7, of which 6 were waited for; matrix products, arithmetic and copies ran while one was open for 28% of the time, Pallas kernels for 0%

commit v1 on v0

v1 whole, which is shorter than its diff:
```python
import jax
import jax.numpy as jnp
from jax import lax
from jax.experimental import pallas as pl
from jax.experimental.pallas import tpu as pltpu
from jax.sharding import PartitionSpec as P

MESH = pl.DeviceIdType.MESH
F32 = jnp.float32
BF16 = jnp.bfloat16
HIGHEST = lax.Precision.HIGHEST

CHUNKS = 4
CHUNK = 128
CAP = 16
REACH = [0, 1, -1, 2, -4, 5, -5, 6, -6, 7, -7, 8, -2, 3, -3, 4]
SLOTS = [(dz, flip) for dz in REACH for flip in (0, 1)]
SLOT_OF = {(dz % 16, flip): k for k, (dz, flip) in enumerate(SLOTS)}


def dot(a, b, precision=None):
    return jnp.dot(a, b, preferred_element_type=F32, precision=precision)


def dot_nt(a, b, precision=None):
    return lax.dot_general(
        a, b, (((1,), (1,)), ((), ())), preferred_element_type=F32, precision=precision
    )


def iota(shape, dim):
    return lax.broadcasted_iota(jnp.int32, shape, dim)


def put(ref, at, value):
    ref[0, at, :] = value[:, :128]
    ref[1, at, :] = value[:, 128:]


def got(ref, at):
    return jnp.concatenate([ref[0, at, :], ref[1, at, :]], axis=1)


class Gather:
    def __init__(self, buf, send, recv, number, place):
        self.buf, self.send, self.recv, self.number = buf, send, recv, number
        self.ep, self.y, self.x = place
        rows = buf.shape[2]
        half, quarter = rows // 2, rows // 4
        y, x = self.y, self.x
        self.xr, self.xl = (x + 1) % 4, (x + 3) % 4
        self.yu, self.yd = (y + 1) % 4, (y + 3) % 4
        xr, xl, yu, yd = self.xr, self.xl, self.yu, self.yd
        a, b = pl.ds(0, half), pl.ds(half, half)
        a0, a1 = pl.ds(0, quarter), pl.ds(quarter, quarter)
        b0, b1 = pl.ds(half, quarter), pl.ds(half + quarter, quarter)
        right, left, up, down = (y, xr), (y, xl), (yu, x), (yd, x)
        self.plan = [
            (buf.at[y, x, a], right),
            (buf.at[y, x, a], left),
            (buf.at[y, x, b], up),
            (buf.at[y, x, b], down),
            (buf.at[y, xl, a0], right),
            (buf.at[y, xr, a1], left),
            (buf.at[yd, x, b0], up),
            (buf.at[yu, x, b1], down),
            (buf.at[y, :, a], up),
            (buf.at[y, :, a], down),
            (buf.at[:, x, b], right),
            (buf.at[:, x, b], left),
            (buf.at[yd, :, a0], up),
            (buf.at[yu, :, a1], down),
            (buf.at[:, xl, b0], right),
            (buf.at[:, xr, b1], left),
        ]

    def copy(self, m):
        ref, (y, x) = self.plan[m]
        return pltpu.make_async_remote_copy(
            src_ref=ref,
            dst_ref=ref,
            send_sem=self.send.at[self.number, m],
            recv_sem=self.recv.at[self.number, m],
            device_id=(self.ep, y * 4 + x),
            device_id_type=MESH,
        )

    def stage(self, s):
        if s == 0:
            for m in range(4):
                self.copy(m).start()
        elif s == 2 or s == 4:
            for m in range(4 * s - 4, 4 * s):
                self.copy(m).wait_recv()
            if s == 2:
                for m in range(8, 12):
                    self.copy(m).start()
        else:
            for m in range(4 * s - 4, 4 * s):
                self.copy(m).wait_recv()
                self.copy(m + 4).start()

    def finish(self):
        for m in range(16):
            self.copy(m).wait_send()


def body(
    x_ref, fac_ref, shift_ref, imap_ref, rout_ref, e_ref, gain_ref, routes_ref, rw_ref,
    mixw_hbm, wg_hbm, wu_hbm, wd_hbm, sg_hbm, su_hbm, sd_hbm,
    mix_ref, exp_ref,
    mixw, wg, wu, wd, sg, su, sd,
    normed, outgoing, sel, rows_buf, hid_buf, res, returned, m_buf, sums,
    push_r, push_i, mag, ph_r, ph_i, keep,
    load_sem, g_send, g_recv, z_send, z_recv, s_send, s_recv, r_send, r_recv,
):
    ep, tp = lax.axis_index("ep"), lax.axis_index("tp")
    z, core = ep // 2, ep % 2
    y, x = tp // 4, tp % 4

    loads = [
        pltpu.make_async_copy(src, dst, load_sem.at[k])
        for k, (src, dst) in enumerate(
            [(sg_hbm, sg), (su_hbm, su), (wg_hbm, wg), (wu_hbm, wu), (wd_hbm, wd),
             (sd_hbm, sd), (mixw_hbm, mixw)]
        )
    ]
    for load in loads:
        load.start()

    def far(dz, flip):
        return ((z + dz + 16) % 16) * 2 + (core + flip) % 2

    barrier = pltpu.get_barrier_semaphore()
    for dz, flip in SLOTS[1:]:
        pl.semaphore_signal(barrier, inc=1, device_id=(far(dz, flip), tp), device_id_type=MESH)
    for ny, nx in ((y, (x + 1) % 4), (y, (x + 3) % 4), ((y + 1) % 4, x), ((y + 3) % 4, x)):
        pl.semaphore_signal(barrier, inc=1, device_id=(ep, ny * 4 + nx), device_id_type=MESH)

    values = e_ref[...].astype(F32)
    scale = lax.rsqrt(jnp.mean(values * values, axis=-1, keepdims=True) + 1e-06)
    normed[...] = (values * scale * gain_ref[...]).astype(BF16)
    lane = iota((128, 128), 1)
    named = [(routes_ref[:, k : k + 1] == lane).astype(F32) for k in (0, 1)]
    earlier = (iota((128, 128), 0) > lane).astype(BF16)
    before = dot(earlier, (named[0] + named[1]).astype(BF16))
    wide = iota((128, 512), 1)
    for k in (0, 1):
        rank = jnp.sum(named[k] * before, axis=1, keepdims=True).astype(jnp.int32)
        sel[k] = (routes_ref[:, k : k + 1] * CAP + rank == wide).astype(BF16)
    own = normed[:, pl.ds(pl.multiple_of(tp * 128, 128), 128)]
    chosen = sel[0].astype(F32) + sel[1].astype(F32)
    outgoing[...] = lax.dot_general(
        chosen.astype(BF16), own, (((0,), (0,)), ((), ())), preferred_element_type=F32
    ).astype(BF16)

    pl.semaphore_wait(barrier, len(SLOTS) - 1 + 4)

    def block_of(k):
        return pl.ds((k % 8) * CAP, CAP)

    def row_send(k):
        dz, flip = SLOTS[k]
        there = SLOT_OF[(-dz % 16, flip)]
        expert = far(dz, flip)
        return pltpu.make_async_remote_copy(
            src_ref=outgoing.at[pl.ds(pl.multiple_of(expert * CAP, CAP), CAP)],
            dst_ref=rows_buf.at[there // 8, y, x, block_of(there)],
            send_sem=z_send,
            recv_sem=z_recv.at[there // 8],
            device_id=(expert, tp),
            device_id_type=MESH,
        )

    for k in range(1, 32):
        row_send(k).start()
    rows_buf[0, y, x, 0:CAP] = outgoing[pl.ds(pl.multiple_of(ep * CAP, CAP), CAP)]

    def rows_arrived(c):
        if c == 0:
            ref = rows_buf.at[0, y, x, pl.ds(CAP, CHUNK - CAP)]
        else:
            ref = rows_buf.at[c, y, x]
        pltpu.make_async_copy(ref, ref, z_recv.at[c]).wait()

    cosine, sine = fac_ref[0:1, :], fac_ref[1:2, :]
    inj_r, inj_i, low = fac_ref[2:3, :], fac_ref[3:4, :], fac_ref[4:5, :]
    spread = (iota((16, 64), 1) % 16 == iota((16, 64), 0)).astype(BF16)
    in_map = dot(imap_ref[...], spread)
    in_map = jnp.where((iota((512, 64), 0) // 64) % 4 == iota((512, 64), 1) // 16, in_map, 0.0)
    drive = dot_nt(x_ref[...], in_map.astype(BF16))
    drive_r, drive_i = drive[:, :256], drive[:, 256:]
    every = slice(None)
    put(push_r, every, inj_r * drive_r - inj_i * drive_i)
    put(push_i, every, inj_r * drive_i + inj_i * drive_r)
    group = iota((256, 256), 1) // 64
    shift = jnp.where(group == 0, shift_ref[:, 0:1], shift_ref[:, 1:2])
    shift = jnp.where(group == 2, shift_ref[:, 2:3], shift)
    shift = jnp.where(group == 3, shift_ref[:, 3:4], shift)
    put(mag, every, jnp.exp(low + shift))
    state_r, state_i = jnp.zeros((8, 256), F32), jnp.zeros((8, 256), F32)
    total = jnp.ones((8, 256), F32)
    turn_r, turn_i = jnp.ones((1, 256), F32), jnp.zeros((1, 256), F32)
    for j in range(32):
        at = pl.ds(j, 8, stride=32)
        m = got(mag, at)
        d_r, d_i = m * cosine, m * sine
        state_r, state_i = (
            d_r * state_r - d_i * state_i + got(push_r, at),
            d_r * state_i + d_i * state_r + got(push_i, at),
        )
        total = total * m
        turn_r, turn_i = turn_r * cosine - turn_i * sine, turn_r * sine + turn_i * cosine
        put(push_r, at, state_r)
        put(push_i, at, state_i)
        put(mag, at, total)
        ph_r[j : j + 1, :] = turn_r
        ph_i[j : j + 1, :] = turn_i
    all_r, all_i = total * turn_r, total * turn_i
    c_r, c_i = jnp.zeros((1, 256), F32), jnp.zeros((1, 256), F32)
    t_r, t_i = jnp.ones((1, 256), F32), jnp.zeros((1, 256), F32)
    for s in range(8):
        for n, part in enumerate((t_r, t_i, c_r, c_i)):
            keep[n, s : s + 1, :] = part
        a_r, a_i = all_r[s : s + 1], all_i[s : s + 1]
        c_r, c_i = (
            a_r * c_r - a_i * c_i + state_r[s : s + 1],
            a_r * c_i + a_i * c_r + state_i[s : s + 1],
        )
        t_r, t_i = a_r * t_r - a_i * t_i, a_r * t_i + a_i * t_r
    for n, part in enumerate((t_r, t_i, c_r, c_i)):
        sums[ep, 2 * n : 2 * n + 1, :] = part[:, :128]
        sums[ep, 2 * n + 1 : 2 * n + 2, :] = part[:, 128:]

    for k in range(1, 32):
        pltpu.make_async_remote_copy(
            src_ref=sums.at[ep],
            dst_ref=sums.at[ep],
            send_sem=s_send,
            recv_sem=s_recv,
            device_id=(far(*SLOTS[k]), tp),
            device_id_type=MESH,
        ).start()

    place = (ep, y, x)
    rows = [Gather(rows_buf.at[c], g_send, g_recv, c, place) for c in range(CHUNKS)]
    hid = [Gather(hid_buf.at[c], g_send, g_recv, CHUNKS + c, place) for c in range(CHUNKS)]
    both = Gather(m_buf, g_send, g_recv, 2 * CHUNKS, place)

    def packed(top, bottom):
        first = (iota((64, 128), 1) == iota((64, 128), 0)).astype(BF16)
        second = (iota((64, 128), 1) == iota((64, 128), 0) + 64).astype(BF16)
        return (dot(top, first) + dot(bottom, second)).astype(BF16)

    def silu(v):
        return v / (1.0 + jnp.exp(-v))

    def shared_part():
        loads[0].wait()
        loads[1].wait()
        hidden = (silu(dot(normed[...], sg[...])) * dot(normed[...], su[...])).astype(BF16)
        m_buf[y, x, 128:192] = packed(hidden[:64], hidden[64:])

    def mixer_part():
        pltpu.make_async_copy(sums.at[pl.ds(0, 31)], sums.at[pl.ds(0, 31)], s_recv).wait()
        in_r, in_i = jnp.zeros((2, 128), F32), jnp.zeros((2, 128), F32)
        for i in range(32):
            a_r, a_i = sums[i, 0:2, :], sums[i, 2:4, :]
            n_r = a_r * in_r - a_i * in_i + sums[i, 4:6, :]
            n_i = a_r * in_i + a_i * in_r + sums[i, 6:8, :]
            in_r, in_i = jnp.where(i < ep, n_r, in_r), jnp.where(i < ep, n_i, in_i)
        in_r = jnp.concatenate([in_r[0:1], in_r[1:2]], axis=1)
        in_i = jnp.concatenate([in_i[0:1], in_i[1:2]], axis=1)
        k_r, k_i = keep[0], keep[1]
        car_r = k_r * in_r - k_i * in_i + keep[2]
        car_i = k_r * in_i + k_i * in_r + keep[3]
        for j in range(32):
            at = pl.ds(j, 8, stride=32)
            p_r, p_i, m = ph_r[j : j + 1, :], ph_i[j : j + 1, :], got(mag, at)
            put(push_r, at, got(push_r, at) + m * (p_r * car_r - p_i * car_i))
            put(push_i, at, got(push_i, at) + m * (p_r * car_i + p_i * car_r))
        spread = (iota((64, 256), 1) % 64 == iota((64, 256), 0)).astype(F32)
        mine = iota((64, 256), 0) // 16 == iota((64, 256), 1) // 64
        out_r = jnp.where(mine, dot(rout_ref[0:64, :], spread, HIGHEST), 0.0)
        out_i = jnp.where(mine, dot(rout_ref[64:128, :], spread, HIGHEST), 0.0)
        every = slice(None)
        v = dot_nt(got(push_r, every), out_r, HIGHEST) - dot_nt(got(push_i, every), out_i, HIGHEST)
        act = 0.5 * v * (1.0 + jnp.tanh(0.7978845608 * (v + 0.044715 * v * v * v)))
        act = act.astype(BF16)
        m_buf[y, x, 0:128] = packed(act[:128], act[128:])

    def joined(ref):
        return jnp.concatenate([ref[s // 4, s % 4] for s in range(16)], axis=1)

    def up_part(c):
        if c == 0:
            loads[2].wait()
            loads[3].wait()
        piece = joined(rows_buf.at[c])
        hid_buf[c, y, x] = (silu(dot(piece, wg[...])) * dot(piece, wu[...])).astype(BF16)

    def down_part(c):
        if c == 0:
            loads[4].wait()
        res[c * CHUNK : (c + 1) * CHUNK] = dot(joined(hid_buf.at[c]), wd[...]).astype(BF16)
        home = pl.ds(pl.multiple_of(ep * CAP, CAP), CAP)
        for k in range(8 * c, 8 * c + 8):
            if k == 0:
                returned[home] = res[0:CAP]
                continue
            pltpu.make_async_remote_copy(
                src_ref=res.at[pl.ds(k * CAP, CAP)],
                dst_ref=returned.at[home],
                send_sem=r_send,
                recv_sem=r_recv,
                device_id=(far(*SLOTS[k]), tp),
                device_id_type=MESH,
            ).start()

    def spread_out(start, height, weight):
        low_half = iota((height, 128), 1) < 64
        total = jnp.zeros((2 * height, 128), F32)
        for s in range(16):
            block = m_buf[s // 4, s % 4, start : start + height]
            zero = jnp.zeros_like(block)
            both_rows = jnp.concatenate(
                [jnp.where(low_half, block, zero), jnp.where(low_half, zero, block)], axis=0
            )
            w = weight[s * 64 : (s + 1) * 64]
            total += dot(both_rows, jnp.concatenate([w, w], axis=0))
        return total

    rows_arrived(0)
    rows[0].stage(0)
    shared_part()
    rows_arrived(1)
    rows[0].stage(1)
    rows[1].stage(0)
    rows_arrived(2)
    rows[0].stage(2)
    rows[1].stage(1)
    rows[2].stage(0)
    rows_arrived(3)
    rows[0].stage(3)
    rows[1].stage(2)
    rows[2].stage(1)
    rows[3].stage(0)
    mixer_part()
    both.stage(0)
    rows[0].stage(4)
    rows[1].stage(3)
    rows[2].stage(2)
    rows[3].stage(1)
    up_part(0)
    hid[0].stage(0)
    both.stage(1)
    rows[1].stage(4)
    rows[2].stage(3)
    rows[3].stage(2)
    up_part(1)
    hid[0].stage(1)
    hid[1].stage(0)
    both.stage(2)
    rows[2].stage(4)
    rows[3].stage(3)
    up_part(2)
    hid[0].stage(2)
    hid[1].stage(1)
    hid[2].stage(0)
    both.stage(3)
    rows[3].stage(4)
    up_part(3)
    hid[0].stage(3)
    hid[1].stage(2)
    hid[2].stage(1)
    hid[3].stage(0)
    both.stage(4)
    loads[5].wait()
    loads[6].wait()
    mix_ref[...] = spread_out(0, 128, mixw).astype(BF16)
    hid[0].stage(4)
    hid[1].stage(3)
    hid[2].stage(2)
    hid[3].stage(1)
    down_part(0)
    hid[1].stage(4)
    hid[2].stage(3)
    hid[3].stage(2)
    down_part(1)
    hid[2].stage(4)
    hid[3].stage(3)
    down_part(2)
    common = spread_out(128, 64, sd)
    hid[3].stage(4)
    down_part(3)

    for gather in rows + hid + [both]:
        gather.finish()
    sent = outgoing.at[pl.ds(0, 31 * CAP)]
    pltpu.make_async_copy(sent, sent, z_send).wait()
    pltpu.make_async_copy(sums.at[pl.ds(0, 31)], sums.at[pl.ds(0, 31)], s_send).wait()
    back = returned.at[pl.ds(0, 31 * CAP)]
    pltpu.make_async_copy(back, back, r_send).wait()
    pltpu.make_async_copy(back, back, r_recv).wait()
    for k in (0, 1):
        common += rw_ref[:, k : k + 1] * dot(sel[k], returned[...])
    exp_ref[...] = common.astype(BF16)


def factors(log_step, states):
    step_rate = jnp.exp(log_step)
    frequency = jnp.pi * jnp.arange(states, dtype=jnp.float32)
    angle = step_rate[:, None] * frequency[None, :]
    turn_cosine = jnp.cos(angle)
    turn_sine = jnp.sin(angle)
    base = jnp.exp(-0.5 * step_rate)[:, None]
    base_real = base * turn_cosine
    starting_quadrature = base * turn_sine
    inverse = 1.0 / (0.25 + frequency * frequency)[None, :]
    lowered = base_real - 1.0
    inject_real = (-0.5 * lowered + starting_quadrature * frequency[None, :]) * inverse
    inject_imaginary = (-0.5 * starting_quadrature - lowered * frequency[None, :]) * inverse
    low = jnp.broadcast_to(-0.5 * step_rate[:, None], angle.shape)
    none = jnp.zeros_like(angle)
    rows = (turn_cosine, turn_sine, inject_real, inject_imaginary, low, none, none, none)
    return jnp.stack([row.reshape(-1) for row in rows])


def shards(
    mixer_input, log_step, decay_shift, input_map, readout, mixer_weight, expert_input,
    norm_gain, routes, route_weight, expert_switch_matrix, up_weight, down_weight,
    shared_gate, shared_up, shared_down,
):
    vmem = pl.BlockSpec(memory_space=pltpu.VMEM)
    hbm = pl.BlockSpec(memory_space=pl.ANY)
    V, DMA = pltpu.VMEM, pltpu.SemaphoreType.DMA
    return pl.pallas_call(
        body,
        out_shape=(
            jax.ShapeDtypeStruct((256, 128), BF16),
            jax.ShapeDtypeStruct((128, 128), BF16),
        ),
        in_specs=[vmem] * 9 + [hbm] * 7,
        out_specs=(vmem, vmem),
        scratch_shapes=[
            V((1024, 128), BF16),
            V((2048, 256), BF16),
            V((2048, 256), BF16),
            V((4096, 128), BF16),
            V((2048, 64), BF16),
            V((2048, 64), BF16),
            V((1024, 128), BF16),
            V((128, 2048), BF16),
            V((512, 128), BF16),
            V((2, 128, 512), BF16),
            V((CHUNKS, 4, 4, CHUNK, 128), BF16),
            V((CHUNKS, 4, 4, CHUNK, 256), BF16),
            V((512, 128), BF16),
            V((512, 128), BF16),
            V((4, 4, 192, 128), BF16),
            V((32, 8, 128), F32),
            V((2, 256, 128), F32),
            V((2, 256, 128), F32),
            V((2, 256, 128), F32),
            V((32, 256), F32),
            V((32, 256), F32),
            V((4, 8, 256), F32),
            DMA((7,)),
            DMA((2 * CHUNKS + 1, 16)),
            DMA((2 * CHUNKS + 1, 16)),
            DMA,
            DMA((CHUNKS,)),
            DMA,
            DMA,
            DMA,
            DMA,
        ],
        compiler_params=pltpu.CompilerParams(
            collective_id=0, has_side_effects=True, vmem_limit_bytes=50 * 1024 * 1024
        ),
    )(
        mixer_input,
        factors(log_step, 64),
        decay_shift,
        input_map.reshape(512, 16),
        readout.reshape(128, 64),
        expert_input,
        norm_gain.reshape(1, 2048),
        routes,
        route_weight,
        mixer_weight,
        expert_switch_matrix[0],
        up_weight[0],
        down_weight[0],
        shared_gate,
        shared_up,
        shared_down,
    )


def solution(mesh):
    placed = (
        P("ep", "tp"),
        P("tp"),
        P("ep", "tp"),
        P(None, "tp", None, None),
        P(None, "tp", None, None),
        P(None, "tp"),
        P("ep", None),
        P(),
        P("ep", None),
        P("ep", None),
        P("ep", None, "tp"),
        P("ep", None, "tp"),
        P("ep", None, "tp"),
        P(None, "tp"),
        P(None, "tp"),
        P(None, "tp"),
    )
    return jax.shard_map(
        shards, mesh=mesh, in_specs=placed, out_specs=(P("ep", "tp"), P("ep", "tp")), check_vma=False
    )
```

time: 235 us -> 97.1 us (0.41)
  Pallas kernels: 0 us -> 88.8 us
  waiting for transfers between devices: 79.2 us -> 0 us
  local copies, waits for them, and re-layouts: 52.1 us -> 7.11 us
  starting transfers between devices: 44.9 us -> 0 us
  other arithmetic: 16.9 us -> 0.09 us
  between operations: 15.8 us -> 0.86 us
  blocking collectives: 12.8 us -> 0 us
  matrix products: 11.7 us -> 0 us
    pallas_call x0 -> x1, Pallas kernels: none -> 88.8 us  [shards(): pl.pallas_call(body, out_shape=(jax.ShapeDtypeStruct((256, 128), BF16), j...]
    all_to_all x5 -> x0, waiting for transfers between devices: 45.9 us -> none  [the longest x3 24.2 us: sent_to_all(): return lax.all_to_all(copies, axis, split_axis=0, concat_axis=0, tiled=True)]
    all_to_all x5 -> x0, starting transfers between devices: 44.8 us -> none  [the longest x3 22 us: sent_to_all(): return lax.all_to_all(copies, axis, split_axis=0, concat_axis=0, tiled=True)]
    slice x143 -> x0, local copies, waits for them, and re-layouts: 37.9 us -> none  [the longest x32 30.6 us: joined_by_halves(): part[side::2]]
    all_gather x2 -> x0, waiting for transfers between devices: 33.3 us -> none  [the longest x1 33.3 us: whole_of(): shard = lax.all_gather(shard, axis, axis=dim, tiled=True)]
    all_gather x1 -> x0, blocking collectives: 12.8 us -> none  [whole_of(): shard = lax.all_gather(shard, axis, axis=dim, tiled=True)]
    dot_general x9 -> x0, matrix products: 11.7 us -> none  [the longest x1 4.43 us: shards(): jnp.dot(lax.all_gather(expert_hidden, TP, axis=1, tiled=True), rows_here,...]
    sub x10 -> x0, other arithmetic: 6 us -> none  [the longest x8 4.81 us: combine_parts(): joint_real = late_real * early_real - late_imaginary * early_imaginary]
  transfers between devices with their start and end apart: 7 -> 0, of which waited for: 6 -> 0; matrix products, arithmetic and copies ran while one was open for 28% -> 0% of each run, Pallas kernels for 0% -> 0%
where the time goes in v1:
time: 97.1 us; the launch traced here: 96.8 us
  Pallas kernels  88.8 us (91%)
  local copies, waits for them, and re-layouts  7.11 us (7%)
    pallas_call x1, Pallas kernels, shards(): pl.pallas_call(body, out_shape=(jax.ShapeDtypeStruct((256, 128), BF16), j...  88.8 us
    unnamed x31, local copies, waits for them, and re-layouts  6.45 us

profile of v1, /device:TPU:1, one launch (start us, length us, event | category | flops | bytes accessed | tf_op | source)
XLA Modules:
  0.0 96.8 jit_solution(5525997072793579035)
XLA Ops:
  0.7 0.0 copy-start.10
  0.7 0.0 copy-start.8
  0.7 0.0 copy-start.9
  0.7 0.0 copy-start.6
  0.7 0.1 mul.213
  0.8 0.1 mul.202
  0.9 0.4 copy-done.10
  1.3 0.1 broadcast_in_dim.2
  1.4 0.1 stack_reshape.4
  1.5 0.1 mul.205
  1.5 0.1 mul.206
  1.6 0.1 mul.197
  1.7 0.1 mul.198
  1.8 0.1 subtract_multiply_fusion
  1.9 0.0 copy-start.7
  1.9 0.0 copy-start
  1.9 1.0 copy.19.x_ref
  2.9 0.0 copy-done.8
  2.9 0.1 copy.21.routes_ref
  3.0 0.0 copy-done.9
  3.0 0.1 copy.22.rw_ref
  3.1 0.0 copy-done.7
  3.1 0.1 copy.20.shift_ref
  3.3 0.9 copy.18
  4.2 0.0 copy-done.6
  4.2 0.0 copy-start.4
  4.2 0.0 copy-start.5
  4.2 0.3 copy.23.sg_hbm
  4.5 0.0 copy-start.1
  4.5 0.0 copy-start.2
  4.5 1.3 %copy.24.su_hbm = bf16[2048,64]{1,0:T(8,128)(2,1)S(1)} copy(bf16[2048,64]{0,1:T(8,128)(2,1)} %param.30) | data formatting | bytes 524288 | tf_op args[14]
  5.8 0.0 copy-done
  5.8 0.0 copy-done.4
  5.8 0.0 copy-done.5
  5.8 0.0 copy-done.1
  5.8 0.0 copy-done.2
  5.9 0.0 copy-start.3
  5.9 0.9 copy-done.3
  6.8 88.8 %shard_map.167 = (bf16[256,128]{1,0:T(8,128)(2,1)S(1)}, bf16[128,128]{1,0:T(8,128)(2,1)S(1)}) custom-call(bf16[256,64]{1,0:T(8,128)(2,1)S(1)} %copy.19.x_ref, f32[8,256]{1,0:T(8,128)S(1)} %stack.7.fac_ref, f32[256,4]{1,0:T(8,128)S(1)} %copy.20.shift_ref, bf16[512,16]{1,0:T(8,128)(2,1)S(1)} %bitcast.7, f32[128,64]{1,0:T(8,128)S(1)} %bitcast.8, ...), custom_call_target="tpu_custom_call" | custom-call | tf_op jit(solution)/shard_map/pallas_call | solution.py:437
  95.6 0.6 copy.27
  96.2 0.6 copy.28
  (8 shorter events, 0.1 us)
Async XLA Ops:
  0.7 0.7 copy-start.10
  0.7 2.2 %copy-start.8 = (s32[128,2]{0,1:T(2,128)S(1)}, s32[128,2]{0,1:T(2,128)}, u32[]{:S(2)}) copy-start(s32[128,2]{0,1:T(2,128)} %param.24) | copy-start | bytes 3076
  0.7 2.3 %copy-start.9 = (f32[128,2]{0,1:T(2,128)S(1)}, f32[128,2]{0,1:T(2,128)}, u32[]{:S(2)}) copy-start(f32[128,2]{0,1:T(2,128)} %param.25) | copy-start | bytes 3076
  0.7 3.5 %copy-start.6 = (bf16[2048,64]{0,1:T(8,128)(2,1)S(1)}, bf16[2048,64]{0,1:T(8,128)(2,1)}, u32[]{:S(2)}) copy-start(bf16[2048,64]{0,1:T(8,128)(2,1)} %param.29) | copy-start | bytes 786436
  1.9 1.3 %copy-start.7 = (f32[256,4]{0,1:T(4,128)S(1)}, f32[256,4]{0,1:T(4,128)}, u32[]{:S(2)}) copy-start(f32[256,4]{0,1:T(4,128)} %param.18) | copy-start | bytes 12292
  1.9 3.9 %copy-start = (bf16[1,2048,256]{2,1,0:T(8,128)(2,1)S(1)}, bf16[1,2048,256]{2,1,0:T(8,128)(2,1)}, u32[]{:S(2)}) copy-start(bf16[1,2048,256]{2,1,0:T(8,128)(2,1)} %param.26) | copy-start | bytes 3145732
  4.2 1.6 %copy-start.4 = (f32[2,4,16,64]{3,2,1,0:T(8,128)S(1)}, f32[2,4,16,64]{3,2,1,0:T(8,128)}, u32[]{:S(2)}) copy-start(f32[2,4,16,64]{3,2,1,0:T(8,128)} %param.20) | copy-start | bytes 98308
  4.2 1.6 %copy-start.5 = (f32[2048]{0:T(1024)S(1)}, f32[2048]{0:T(1024)}, u32[]{:S(2)}) copy-start(f32[2048]{0:T(1024)} %param.23) | copy-start | bytes 24580
  4.5 1.4 %copy-start.1 = (bf16[128,2048]{1,0:T(8,128)(2,1)S(1)}, bf16[128,2048]{1,0:T(8,128)(2,1)}, u32[]{:S(2)}) copy-start(bf16[128,2048]{1,0:T(8,128)(2,1)} %e_ref.1) | copy-start | bytes 1572868
  4.5 1.4 %copy-start.2 = (bf16[1024,128]{1,0:T(8,128)(2,1)S(1)}, bf16[1024,128]{1,0:T(8,128)(2,1)}, u32[]{:S(2)}) copy-start(bf16[1024,128]{1,0:T(8,128)(2,1)} %mixw_hbm.1) | copy-start | bytes 786436
  5.9 1.0 copy-start.3

commit v2 on v1

v2 whole, which is shorter than its diff:
```python
import jax
import jax.numpy as jnp
from jax import lax
from jax.experimental import pallas as pl
from jax.experimental.pallas import tpu as pltpu
from jax.sharding import PartitionSpec as P

MESH = pl.DeviceIdType.MESH
F32 = jnp.float32
BF16 = jnp.bfloat16
HIGHEST = lax.Precision.HIGHEST

CHUNKS = 4
CHUNK = 128
CAP = 16
REACH = [0, 1, -1, 2, -4, 5, -5, 6, -6, 7, -7, 8, -2, 3, -3, 4]
SLOTS = [(dz, flip) for dz in REACH for flip in (0, 1)]
SLOT_OF = {(dz % 16, flip): k for k, (dz, flip) in enumerate(SLOTS)}


def dot(a, b, precision=None):
    return jnp.dot(a, b, preferred_element_type=F32, precision=precision)


def dot_nt(a, b, precision=None):
    return lax.dot_general(
        a, b, (((1,), (1,)), ((), ())), preferred_element_type=F32, precision=precision
    )


def dot_tn(a, b, precision=None):
    return lax.dot_general(
        a, b, (((0,), (0,)), ((), ())), preferred_element_type=F32, precision=precision
    )


def iota(shape, dim):
    return lax.broadcasted_iota(jnp.int32, shape, dim)


def put(ref, at, value):
    ref[0, at, :] = value[:, :128]
    ref[1, at, :] = value[:, 128:]


def got(ref, at):
    return jnp.concatenate([ref[0, at, :], ref[1, at, :]], axis=1)


PASSED_ON = {0: 0, 1: 1, 2: 2, 3: 3, 4: 4, 5: 5, 6: 6, 7: 7, 8: 8, 9: 9}
PASSED_ON = {**PASSED_ON, 12: 21, 13: 22}


class Gather:
    def __init__(self, buf, send, recv, number, place):
        self.buf, self.send, self.recv, self.number = buf, send, recv, number
        self.ep, self.y, self.x = place
        self.half = buf.shape[1] // 2
        self.plan = []
        for turned in (False, True):
            messages = [(0, 0, None, 0, 1), (0, 0, None, 0, -1), (0, 0, None, 1, 1), (0, 0, None, 1, -1)]
            messages += [(-1, 0, 0, 0, 1), (1, 0, 1, 0, -1)]
            messages += [(i, 0, None, 1, d) for i in (-1, 1) for d in (1, -1)]
            messages += [(0, -1, 0, 1, 1), (0, 1, 1, 1, -1)]
            messages += [(2, 0, None, 1, 1), (2, 0, None, 1, -1)]
            messages += [(i, -d, (1 - d) // 2, 1, d) for i in (-1, 1) for d in (1, -1)]
            messages += [(2, -1, 0, 1, 1), (2, 1, 1, 1, -1)]
            self.plan += [(turned, *m) for m in messages]

    def copy(self, m):
        turned, i, j, part, ring, step = self.plan[m]
        dy, dx = (i, j) if turned else (j, i)
        shard = ((self.y + dy + 4) % 4) * 4 + (self.x + dx + 4) % 4
        start, count = (self.half if turned else 0), self.half
        if part is not None:
            count = self.half // 2
            start += part * count
        along_y = (ring == 0) == turned
        ny = (self.y + step + 4) % 4 if along_y else self.y
        nx = self.x if along_y else (self.x + step + 4) % 4
        ref = self.buf.at[shard, pl.ds(start, count)]
        stage = sum(m % 20 >= first for first in (4, 12, 18))
        arrival = PASSED_ON.get(m % 20)
        arrival = 20 if arrival is None else arrival + (2 if arrival > 20 else 10) * (m // 20)
        return pltpu.make_async_remote_copy(
            src_ref=ref,
            dst_ref=ref,
            send_sem=self.send.at[self.number, stage],
            recv_sem=self.recv.at[self.number, arrival],
            device_id=(self.ep, ny * 4 + nx),
            device_id_type=MESH,
        )

    def whole(self, count, sem):
        ref = self.buf.at[pl.ds(0, count)]
        pltpu.make_async_copy(ref, ref, sem).wait()

    def stage(self, s):
        with jax.named_scope(f"g{self.number}s{s}"):
            if s == 4:
                self.whole(4, self.recv.at[self.number, 20])
                return
            then = [
                [(None, (0, 1, 2, 3))],
                [(0, (4, 6, 7)), (1, (5, 8, 9)), (2, (10,)), (3, (11,))],
                [(4, ()), (5, (12, 13)), (6, (14,)), (7, (15,)), (8, (16,)), (9, (17,))],
                [(12, (18,)), (13, (19,))],
            ][s]
            for wait, starts in then:
                for turn in (0, 20):
                    if wait is not None:
                        self.copy(turn + wait).wait_recv()
                    for m in starts:
                        self.copy(turn + m).start()

    def finish(self):
        for stage, count in enumerate((4, 6, 4, 1)):
            self.whole(count, self.send.at[self.number, stage])


def factors(log_step, state):
    step_rate = jnp.exp(log_step)
    frequency = jnp.pi * state.astype(F32)
    angle = step_rate * frequency
    turn_cosine = jnp.cos(angle)
    turn_sine = jnp.sin(angle)
    base = jnp.exp(-0.5 * step_rate)
    base_real = base * turn_cosine
    starting_quadrature = base * turn_sine
    inverse = 1.0 / (0.25 + frequency * frequency)
    lowered = base_real - 1.0
    inject_real = (-0.5 * lowered + starting_quadrature * frequency) * inverse
    inject_imaginary = (-0.5 * starting_quadrature - lowered * frequency) * inverse
    return (turn_cosine, turn_sine, inject_real, inject_imaginary, -0.5 * step_rate)


def body(
    step_ref, x_hbm, shift_hbm, imap_hbm, rout_hbm, e_hbm, gain_hbm, routes_hbm, rw_hbm,
    mixw_hbm, wg_hbm, wu_hbm, wd_hbm, sg_hbm, su_hbm, sd_hbm,
    mix_ref, exp_ref,
    x_ref, shift_ref, imap_ref, rout_ref, e_ref, gain_ref, routes_ref, rw_ref, mixw, wg, wu, wd, sgu, sd,
    normed, outgoing, back_hi, back_lo, rows_buf, hid_buf, res, returned, mix_buf, sh_buf, pair, chips,
    push_r, push_i, mag, ph_r, ph_i, keep,
    load_sem, g_send, g_recv, z_send, z_recv, s_send, s_recv, r_send, r_recv,
):
    ep, tp = lax.axis_index("ep"), lax.axis_index("tp")
    z, core = ep // 2, ep % 2
    y, x = tp // 4, tp % 4

    loads = [
        pltpu.make_async_copy(src, dst, load_sem.at[k])
        for k, (src, dst) in enumerate(
            [(sg_hbm, sgu.at[0:64]), (su_hbm, sgu.at[64:128]), (wg_hbm, wg), (wu_hbm, wu),
             (wd_hbm, wd), (sd_hbm, sd), (mixw_hbm, mixw), (e_hbm, e_ref), (gain_hbm, gain_ref),
             (routes_hbm, routes_ref), (x_hbm, x_ref), (shift_hbm, shift_ref),
             (imap_hbm, imap_ref), (rout_hbm, rout_ref), (rw_hbm, rw_ref)]
        )
    ]
    for k in (7, 8, 9, 10, 11, 12, 13, 14, 0, 1, 2, 3, 4, 5, 6):
        loads[k].start()

    def far(dz, flip):
        return ((z + dz + 16) % 16) * 2 + (core + flip) % 2

    chips[...] = jnp.zeros_like(chips)
    barrier = pltpu.get_barrier_semaphore()
    for dz, flip in SLOTS[1:]:
        pl.semaphore_signal(barrier, inc=1, device_id=(far(dz, flip), tp), device_id_type=MESH)
    for ny, nx in ((y, (x + 1) % 4), (y, (x + 3) % 4), ((y + 1) % 4, x), ((y + 3) % 4, x)):
        pl.semaphore_signal(barrier, inc=1, device_id=(ep, ny * 4 + nx), device_id_type=MESH)

    with jax.named_scope("load"):
        for k in (7, 8, 9):
            loads[k].wait()
    values = e_ref[...].astype(F32)
    scale = lax.rsqrt(jnp.mean(values * values, axis=-1, keepdims=True) + 1e-06)
    normed[...] = (values * scale * gain_ref[...]).astype(BF16)
    expert = iota((32, 128), 0)
    named = [(routes_ref[k : k + 1, :] == expert).astype(F32) for k in (0, 1)]
    earlier = (iota((128, 128), 0) < iota((128, 128), 1)).astype(BF16)
    before = dot((named[0] + named[1]).astype(BF16), earlier)
    slot = iota((512, 128), 0)
    took = []
    for k in (0, 1):
        rank = jnp.sum(named[k] * before, axis=0, keepdims=True).astype(jnp.int32)
        took.append((routes_ref[k : k + 1, :] * CAP + rank == slot).astype(F32))
    own = normed[:, pl.ds(pl.multiple_of(tp * 128, 128), 128)]
    outgoing[...] = dot((took[0] + took[1]).astype(BF16), own).astype(BF16)

    with jax.named_scope("enter"):
        pl.semaphore_wait(barrier, len(SLOTS) - 1 + 4)

    def block_of(k):
        return pl.ds((k % 8) * CAP, CAP)

    def row_send(k):
        dz, flip = SLOTS[k]
        there = SLOT_OF[(-dz % 16, flip)]
        expert = far(dz, flip)
        return pltpu.make_async_remote_copy(
            src_ref=outgoing.at[pl.ds(pl.multiple_of(expert * CAP, CAP), CAP)],
            dst_ref=rows_buf.at[there // 8, tp, block_of(there)],
            send_sem=z_send,
            recv_sem=z_recv.at[there // 8],
            device_id=(expert, tp),
            device_id_type=MESH,
        )

    def send_chunk(c):
        for k in range(1, 32):
            dz, flip = SLOTS[k]
            if SLOT_OF[(-dz % 16, flip)] // 8 == c:
                row_send(k).start()

    send_chunk(0)
    rows_buf[0, tp, 0:CAP] = outgoing[pl.ds(pl.multiple_of(ep * CAP, CAP), CAP)]

    def rows_arrived(c):
        if c == 0:
            ref = rows_buf.at[0, tp, pl.ds(CAP, CHUNK - CAP)]
        else:
            ref = rows_buf.at[c, tp]
        pltpu.make_async_copy(ref, ref, z_recv.at[c]).wait()

    def to_partner():
        return pltpu.make_async_remote_copy(
            src_ref=pair.at[core],
            dst_ref=pair.at[core],
            send_sem=s_send.at[0],
            recv_sem=s_recv.at[0],
            device_id=(far(0, 1), tp),
            device_id_type=MESH,
        )

    def to_chip(dz):
        return pltpu.make_async_remote_copy(
            src_ref=chips.at[z],
            dst_ref=chips.at[z],
            send_sem=s_send.at[dz],
            recv_sem=s_recv.at[dz],
            device_id=(far(dz, 0), tp),
            device_id_type=MESH,
        )

    def parts_of(ref, i):
        return [ref[i, 2 * n : 2 * n + 2, :] for n in range(4)]

    def after(early_r, early_i, late):
        a_r, a_i, c_r, c_i = late
        return a_r * early_r - a_i * early_i + c_r, a_r * early_i + a_i * early_r + c_i

    def pair_part():
        to_partner().wait_recv()
        first, second = parts_of(pair, 0), parts_of(pair, 1)
        a_r, a_i = first[0] * second[0] - first[1] * second[1], first[0] * second[1] + first[1] * second[0]
        c_r, c_i = after(first[2], first[3], second)
        for n, part in enumerate((a_r, a_i, c_r, c_i)):
            chips[z, 2 * n : 2 * n + 2, :] = part
        for dz in range(1, 16):

            @pl.when(z + dz < 16)
            def _(dz=dz):
                to_chip(dz).start()

    def scan_part():
        with jax.named_scope("load2"):
            for k in (10, 11, 12):
                loads[k].wait()
        group = iota((1, 256), 1) // 64
        log_step = jnp.where(group == 0, step_ref[0], step_ref[1])
        log_step = jnp.where(group == 2, step_ref[2], log_step)
        log_step = jnp.where(group == 3, step_ref[3], log_step)
        cosine, sine, inj_r, inj_i, low = factors(log_step, iota((1, 256), 1) % 64)
        spread = (iota((64, 256), 1) % 64 == iota((64, 256), 0)).astype(BF16)
        mine = iota((64, 256), 0) // 16 == iota((64, 256), 1) // 64
        drive_r, drive_i = [
            dot_tn(
                x_ref[...],
                jnp.where(mine, dot(imap_ref[64 * c : 64 * c + 64, :], spread), 0.0).astype(BF16),
            )
            for c in (0, 1)
        ]
        every = slice(None)
        put(push_r, every, inj_r * drive_r - inj_i * drive_i)
        put(push_i, every, inj_r * drive_i + inj_i * drive_r)
        of_group = (iota((4, 256), 1) // 64 == iota((4, 256), 0)).astype(F32)
        put(mag, every, jnp.exp(low + dot_tn(shift_ref[...], of_group, HIGHEST)))
        state_r, state_i = jnp.zeros((8, 256), F32), jnp.zeros((8, 256), F32)
        total = jnp.ones((8, 256), F32)
        turn_r, turn_i = jnp.ones((1, 256), F32), jnp.zeros((1, 256), F32)
        for j in range(32):
            at = pl.ds(j, 8, stride=32)
            m = got(mag, at)
            d_r, d_i = m * cosine, m * sine
            state_r, state_i = (
                d_r * state_r - d_i * state_i + got(push_r, at),
                d_r * state_i + d_i * state_r + got(push_i, at),
            )
            total = total * m
            turn_r, turn_i = turn_r * cosine - turn_i * sine, turn_r * sine + turn_i * cosine
            put(push_r, at, state_r)
            put(push_i, at, state_i)
            put(mag, at, total)
            ph_r[j : j + 1, :] = turn_r
            ph_i[j : j + 1, :] = turn_i
        all_r, all_i = total * turn_r, total * turn_i
        c_r, c_i = jnp.zeros((1, 256), F32), jnp.zeros((1, 256), F32)
        t_r, t_i = jnp.ones((1, 256), F32), jnp.zeros((1, 256), F32)
        for s in range(8):
            for n, part in enumerate((t_r, t_i, c_r, c_i)):
                keep[n, s : s + 1, :] = part
            a_r, a_i = all_r[s : s + 1], all_i[s : s + 1]
            c_r, c_i = (
                a_r * c_r - a_i * c_i + state_r[s : s + 1],
                a_r * c_i + a_i * c_r + state_i[s : s + 1],
            )
            t_r, t_i = a_r * t_r - a_i * t_i, a_r * t_i + a_i * t_r
        for n, part in enumerate((t_r, t_i, c_r, c_i)):
            pair[core, 2 * n : 2 * n + 1, :] = part[:, :128]
            pair[core, 2 * n + 1 : 2 * n + 2, :] = part[:, 128:]
        to_partner().start()

    place = (ep, y, x)
    rows = [Gather(rows_buf.at[c], g_send, g_recv, c, place) for c in range(CHUNKS)]
    hid = [Gather(hid_buf.at[c], g_send, g_recv, CHUNKS + c, place) for c in range(CHUNKS)]
    mixed = Gather(mix_buf, g_send, g_recv, 2 * CHUNKS, place)
    shared = Gather(sh_buf, g_send, g_recv, 2 * CHUNKS + 1, place)

    def packed(top, bottom):
        first = (iota((64, 128), 1) == iota((64, 128), 0)).astype(BF16)
        second = (iota((64, 128), 1) == iota((64, 128), 0) + 64).astype(BF16)
        return (dot(top, first) + dot(bottom, second)).astype(BF16)

    def silu(v):
        return v / (1.0 + jnp.exp(-v))

    def shared_part():
        loads[0].wait()
        loads[1].wait()
        both_sums = dot_nt(normed[...], sgu[...])
        hidden = (silu(both_sums[:, :64]) * both_sums[:, 64:]).astype(BF16)
        sh_buf[tp] = packed(hidden[:64], hidden[64:])

    def mixer_part():
        with jax.named_scope("sums"):
            for dz in range(1, 16):

                @pl.when(z - dz >= 0)
                def _(dz=dz):
                    to_chip(dz).wait_recv()

        in_r, in_i = jnp.zeros((2, 128), F32), jnp.zeros((2, 128), F32)
        for i in range(15):
            n_r, n_i = after(in_r, in_i, parts_of(chips, i))
            in_r, in_i = jnp.where(i < z, n_r, in_r), jnp.where(i < z, n_i, in_i)
        n_r, n_i = after(in_r, in_i, parts_of(pair, 0))
        in_r, in_i = jnp.where(core == 1, n_r, in_r), jnp.where(core == 1, n_i, in_i)
        in_r = jnp.concatenate([in_r[0:1], in_r[1:2]], axis=1)
        in_i = jnp.concatenate([in_i[0:1], in_i[1:2]], axis=1)
        k_r, k_i = keep[0], keep[1]
        car_r = k_r * in_r - k_i * in_i + keep[2]
        car_i = k_r * in_i + k_i * in_r + keep[3]
        for j in range(32):
            at = pl.ds(j, 8, stride=32)
            p_r, p_i, m = ph_r[j : j + 1, :], ph_i[j : j + 1, :], got(mag, at)
            put(push_r, at, got(push_r, at) + m * (p_r * car_r - p_i * car_i))
            put(push_i, at, got(push_i, at) + m * (p_r * car_i + p_i * car_r))
        loads[13].wait()
        spread = (iota((64, 256), 1) % 64 == iota((64, 256), 0)).astype(F32)
        mine = iota((64, 256), 0) // 16 == iota((64, 256), 1) // 64
        out_r = jnp.where(mine, dot(rout_ref[0:64, :], spread, HIGHEST), 0.0)
        out_i = jnp.where(mine, dot(rout_ref[64:128, :], spread, HIGHEST), 0.0)
        every = slice(None)
        v = dot_nt(got(push_r, every), out_r, HIGHEST) - dot_nt(got(push_i, every), out_i, HIGHEST)
        act = 0.5 * v * (1.0 + jnp.tanh(0.7978845608 * (v + 0.044715 * v * v * v)))
        act = act.astype(BF16)
        mix_buf[tp] = packed(act[:128], act[128:])

    def joined(ref):
        return jnp.concatenate([ref[s] for s in range(16)], axis=1)

    def up_part(c):
        if c == 0:
            loads[2].wait()
            loads[3].wait()
        piece = joined(rows_buf.at[c])
        hid_buf[c, tp] = (silu(dot(piece, wg[...])) * dot(piece, wu[...])).astype(BF16)

    def down_part(c):
        if c == 0:
            loads[4].wait()
        res[c * CHUNK : (c + 1) * CHUNK] = dot(joined(hid_buf.at[c]), wd[...]).astype(BF16)
        home = pl.ds(pl.multiple_of(ep * CAP, CAP), CAP)
        for k in range(8 * c, 8 * c + 8):
            if k == 0:
                returned[home] = res[0:CAP]
                continue
            pltpu.make_async_remote_copy(
                src_ref=res.at[pl.ds(k * CAP, CAP)],
                dst_ref=returned.at[home],
                send_sem=r_send,
                recv_sem=r_recv,
                device_id=(far(*SLOTS[k]), tp),
                device_id_type=MESH,
            ).start()

    def spread_out(buf, weight):
        height = buf.shape[1]
        low_half = iota((height, 128), 1) < 64
        total = jnp.zeros((2 * height, 128), F32)
        for s in range(16):
            block = buf[s]
            zero = jnp.zeros_like(block)
            both_rows = jnp.concatenate(
                [jnp.where(low_half, block, zero), jnp.where(low_half, zero, block)], axis=0
            )
            w = weight[s * 64 : (s + 1) * 64]
            total += dot(both_rows, jnp.concatenate([w, w], axis=0))
        return total

    def arrive(c):
        with jax.named_scope(f"arrive{c}"):
            rows_arrived(c)
        rows[c].stage(0)

    def up(c):
        rows[c].stage(4)
        with jax.named_scope(f"up{c}"):
            up_part(c)
        hid[c].stage(0)

    def down(c):
        with jax.named_scope(f"down{c}"):
            down_part(c)

    with jax.named_scope("shared_part"):
        shared_part()
    arrive(0)
    for c in (1, 2, 3):
        send_chunk(c)
    shared.stage(0)
    with jax.named_scope("scan"):
        scan_part()
    rows[0].stage(1)
    shared.stage(1)
    loads[14].wait()
    weighted = jnp.transpose(took[0] * rw_ref[0:1, :] + took[1] * rw_ref[1:2, :])
    rounded = weighted.astype(BF16)
    back_hi[...] = rounded
    back_lo[...] = (weighted - rounded.astype(F32)).astype(BF16)
    with jax.named_scope("pair"):
        pair_part()
    rows[0].stage(2)
    shared.stage(2)
    arrive(1)
    rows[0].stage(3)
    shared.stage(3)
    arrive(2)
    rows[1].stage(1)
    up(0)
    shared.stage(4)
    arrive(3)
    rows[2].stage(1)
    rows[1].stage(2)
    hid[0].stage(1)
    with jax.named_scope("mixer_part"):
        mixer_part()
    mixed.stage(0)
    rows[3].stage(1)
    rows[2].stage(2)
    rows[1].stage(3)
    hid[0].stage(2)
    mixed.stage(1)
    up(1)
    rows[2].stage(3)
    rows[3].stage(2)
    hid[0].stage(3)
    mixed.stage(2)
    up(2)
    rows[3].stage(3)
    hid[1].stage(1)
    hid[0].stage(4)
    mixed.stage(3)
    up(3)
    hid[1].stage(2)
    hid[2].stage(1)
    down(0)
    mixed.stage(4)
    hid[1].stage(3)
    hid[2].stage(2)
    hid[3].stage(1)
    loads[5].wait()
    loads[6].wait()
    mix_ref[...] = spread_out(mix_buf, mixw).astype(BF16)
    hid[1].stage(4)
    hid[2].stage(3)
    hid[3].stage(2)
    down(1)
    hid[2].stage(4)
    hid[3].stage(3)
    down(2)
    common = spread_out(sh_buf, sd)
    hid[3].stage(4)
    down(3)

    with jax.named_scope("finish"):
        for gather in rows + hid + [mixed, shared]:
            gather.finish()
        to_partner().wait_send()
        for dz in range(1, 16):

            @pl.when(z + dz < 16)
            def _(dz=dz):
                to_chip(dz).wait_send()

    sent = outgoing.at[pl.ds(0, 31 * CAP)]
    pltpu.make_async_copy(sent, sent, z_send).wait()
    back = returned.at[pl.ds(0, 31 * CAP)]
    pltpu.make_async_copy(back, back, r_send).wait()
    with jax.named_scope("last"):
        pltpu.make_async_copy(back, back, r_recv).wait()
    common += dot(back_hi[...], returned[...]) + dot(back_lo[...], returned[...])
    exp_ref[...] = common.astype(BF16)


def shards(
    mixer_input, log_step, decay_shift, input_map, readout, mixer_weight, expert_input,
    norm_gain, routes, route_weight, expert_switch_matrix, up_weight, down_weight,
    shared_gate, shared_up, shared_down,
):
    vmem = pl.BlockSpec(memory_space=pltpu.VMEM)
    hbm = pl.BlockSpec(memory_space=pltpu.HBM)
    V, DMA = pltpu.VMEM, pltpu.SemaphoreType.DMA
    return pl.pallas_call(
        body,
        out_shape=(
            jax.ShapeDtypeStruct((256, 128), BF16),
            jax.ShapeDtypeStruct((128, 128), BF16),
        ),
        in_specs=[pl.BlockSpec(memory_space=pltpu.SMEM)] + [hbm] * 15,
        out_specs=(vmem, vmem),
        scratch_shapes=[
            V((64, 256), BF16),
            V((4, 256), F32),
            V((128, 64), BF16),
            V((128, 64), F32),
            V((128, 2048), BF16),
            V((1, 2048), F32),
            V((2, 128), jnp.int32),
            V((2, 128), F32),
            V((1024, 128), BF16),
            V((2048, 256), BF16),
            V((2048, 256), BF16),
            V((4096, 128), BF16),
            V((128, 2048), BF16),
            V((1024, 128), BF16),
            V((128, 2048), BF16),
            V((512, 128), BF16),
            V((128, 512), BF16),
            V((128, 512), BF16),
            V((CHUNKS, 16, CHUNK, 128), BF16),
            V((CHUNKS, 16, CHUNK, 256), BF16),
            V((512, 128), BF16),
            V((512, 128), BF16),
            V((16, 128, 128), BF16),
            V((16, 64, 128), BF16),
            V((2, 8, 128), F32),
            V((16, 8, 128), F32),
            V((2, 256, 128), F32),
            V((2, 256, 128), F32),
            V((2, 256, 128), F32),
            V((32, 256), F32),
            V((32, 256), F32),
            V((4, 8, 256), F32),
            DMA((15,)),
            DMA((2 * CHUNKS + 2, 4)),
            DMA((2 * CHUNKS + 2, 25)),
            DMA,
            DMA((CHUNKS,)),
            DMA((16,)),
            DMA((16,)),
            DMA,
            DMA,
        ],
        compiler_params=pltpu.CompilerParams(
            collective_id=0, has_side_effects=True, vmem_limit_bytes=67_043_328
        ),
    )(
        log_step,
        mixer_input.T,
        decay_shift.T,
        jnp.swapaxes(input_map, 2, 3).reshape(128, 64),
        readout.reshape(128, 64),
        expert_input,
        norm_gain.reshape(1, 2048),
        routes.T,
        route_weight.T,
        mixer_weight,
        expert_switch_matrix[0],
        up_weight[0],
        down_weight[0],
        shared_gate.T,
        shared_up.T,
        shared_down,
    )


def solution(mesh):
    placed = (
        P("ep", "tp"),
        P("tp"),
        P("ep", "tp"),
        P(None, "tp", None, None),
        P(None, "tp", None, None),
        P(None, "tp"),
        P("ep", None),
        P(),
        P("ep", None),
        P("ep", None),
        P("ep", None, "tp"),
        P("ep", None, "tp"),
        P("ep", None, "tp"),
        P(None, "tp"),
        P(None, "tp"),
        P(None, "tp"),
    )
    return jax.shard_map(
        shards, mesh=mesh, in_specs=placed, out_specs=(P("ep", "tp"), P("ep", "tp")), check_vma=False
    )
```

time: 97.1 us -> 87.8 us (0.904)
  local copies, waits for them, and re-layouts: 7.11 us -> 2.1 us
  Pallas kernels: 88.8 us -> 84.9 us
    unnamed x31 -> x4, local copies, waits for them, and re-layouts: 6.45 us -> 2.1 us
    pallas_call x1, Pallas kernels: 88.8 us -> 84.9 us  [shards(): pl.pallas_call(body, out_shape=(jax.ShapeDtypeStruct((256, 128), BF16), j...]
where the time goes in v2:
time: 87.8 us; the launch traced here: 87.6 us
  Pallas kernels  84.9 us (97%)
  local copies, waits for them, and re-layouts  2.1 us (2%)
    pallas_call x1, Pallas kernels, shards(): pl.pallas_call(body, out_shape=(jax.ShapeDtypeStruct((256, 128), BF16), j...  84.9 us
    unnamed x4, local copies, waits for them, and re-layouts  2.1 us

profile of v2, /device:TPU:1, one launch (start us, length us, event | category | flops | bytes accessed | tf_op | source)
XLA Modules:
  0.0 87.6 jit_solution(9789553066321597595)
XLA Ops:
  0.6 84.9 %shard_map.167 = (bf16[256,128]{1,0:T(8,128)(2,1)}, bf16[128,128]{1,0:T(8,128)(2,1)}) custom-call(f32[4]{0:T(128)} %step_ref.1, bf16[64,256]{1,0:T(8,128)(2,1)} %bitcast.20, f32[4,256]{1,0:T(4,128)} %bitcast.23, bf16[128,64]{1,0:T(8,128)(2,1)} %bitcast.21, f32[128,64]{1,0:T(8,128)} %bitcast.19, bf16[128,2048]{1,0:T(8,128)(2,1)} %e_hbm.1, ...), custom_call_target="tpu_custom_call" | custom-call | tf_op jit(solution)/shard_map/pallas_call | solution.py:534
  85.5 0.0 copy-start
  85.5 1.5 %copy.20 = bf16[256,128]{1,0:T(8,128)(2,1)} copy(bf16[256,128]{1,0:T(8,128)(2,1)} %get-tuple-element.4) | data formatting | bytes 131072
  87.0 0.0 copy-done
  87.0 0.6 copy.21
Async XLA Ops:
  85.5 1.5 %copy-start = (bf16[128,128]{1,0:T(8,128)(2,1)S(1)}, bf16[128,128]{1,0:T(8,128)(2,1)}, u32[]{:S(2)}) copy-start(bf16[128,128]{1,0:T(8,128)(2,1)} %get-tuple-element.5) | copy-start | bytes 98308

commit v3 on v2

--- a/solution.py
+++ b/solution.py
@@ -1,3 +1,5 @@
+import heapq
+
 import jax
 import jax.numpy as jnp
 from jax import lax
@@ -15,7 +17,6 @@
 CAP = 16
 REACH = [0, 1, -1, 2, -4, 5, -5, 6, -6, 7, -7, 8, -2, 3, -3, 4]
 SLOTS = [(dz, flip) for dz in REACH for flip in (0, 1)]
-SLOT_OF = {(dz % 16, flip): k for k, (dz, flip) in enumerate(SLOTS)}
 
 
 def dot(a, b, precision=None):
@@ -47,8 +48,69 @@
     return jnp.concatenate([ref[0, at, :], ref[1, at, :]], axis=1)
 
 
-PASSED_ON = {0: 0, 1: 1, 2: 2, 3: 3, 4: 4, 5: 5, 6: 6, 7: 7, 8: 8, 9: 9}
-PASSED_ON = {**PASSED_ON, 12: 21, 13: 22}
+THEN = {0: (4, 6, 7), 1: (5, 8, 9), 2: (10,), 3: (11,), 4: (), 5: (12, 13)}
+THEN = {**THEN, 6: (14,), 7: (15,), 8: (16,), 9: (17,), 12: (18,), 13: (19,)}
+PLACE = {**{m: m for m in range(10)}, 12: 21, 13: 22}
+WHOLE = (0, 1, 2, 3, 6, 7, 8, 9, 12, 13)
+RING = [0, 0, 1, 1, 0, 0] + [1] * 14
+BACKWARD = [0, 1] * 10
+
+
+def schedule(hop=1.9, rate=46600.0, later=(0.0, 7.0, 7.0, 7.0), mixer_at=14.0):
+    size = {("shared", 0): 16384, ("mixed", 0): 32768}
+    rank = {("shared", 0): 0.5, ("mixed", 0): 1.5}
+    for c in range(CHUNKS):
+        size["rows", c], size["hid", c] = 32768, 65536
+        rank["rows", c] = rank["hid", c] = c
+    cost = {"scan": 2.2, "pair": 0.1, "back": 0.5, "mixer": 1.9, "mix_out": 0.6, "up": 0.47, "down": 0.47}
+    urgency = {"up": 1, "down": 2, "scan": 3, "pair": 3, "back": 4, "mixer": 3, "mix_out": 4}
+    now, free = 0.0, [0.0] * 4
+    coming, ready, events = [], [], []
+    ends = {gather: [] for gather in size}
+    seen = {gather: 0 for gather in size}
+
+    def send(gather, turn, m):
+        nonlocal now
+        now += 0.007
+        link = (RING[m] ^ turn) * 2 + BACKWARD[m]
+        free[link] = max(now, free[link]) + size[gather] / (2 if m in WHOLE else 4) / rate
+        if m in THEN:
+            heapq.heappush(coming, (free[link] + hop, rank[gather], ("message", gather, turn, m)))
+            return
+        ends[gather].append(free[link] + hop)
+        if len(ends[gather]) == 16:
+            heapq.heappush(coming, (max(ends[gather]), rank[gather], ("leaves", gather)))
+
+    def begin(gather):
+        for m in range(4):
+            for turn in (0, 1):
+                send(gather, turn, m)
+
+    for c in range(CHUNKS):
+        heapq.heappush(coming, (later[c], 0.0, ("arrive", c)))
+    for at, name in ((0.0, "shared"), (0.0, "scan"), (4.5, "pair"), (5.0, "back"), (mixer_at, "mixer")):
+        heapq.heappush(coming, (at, 1.5, (name, 0)))
+    while coming or ready:
+        while coming and (coming[0][0] <= now or not ready):
+            at, order, event = heapq.heappop(coming)
+            now = max(now, at)
+            heapq.heappush(ready, (urgency.get(event[0], 0), order, at, event))
+        event = heapq.heappop(ready)[3]
+        events.append(event)
+        now += cost.get(event[0], 0.01)
+        name, which = event[:2]
+        if name in ("arrive", "shared", "mixer", "up"):
+            begin(({"arrive": "rows", "up": "hid", "mixer": "mixed"}.get(name, name), which))
+        if name in ("message", "leaves"):
+            if name == "message":
+                for m in THEN[event[3]]:
+                    send(which, event[2], m)
+            seen[which] += 1
+            if seen[which] == 25:
+                last = {"rows": "up", "hid": "down", "mixed": "mix_out"}.get(which[0])
+                if last:
+                    heapq.heappush(ready, (urgency[last], rank[which], now, (last, which[1])))
+    return events
 
 
 class Gather:
@@ -80,7 +142,7 @@
         nx = self.x if along_y else (self.x + step + 4) % 4
         ref = self.buf.at[shard, pl.ds(start, count)]
         stage = sum(m % 20 >= first for first in (4, 12, 18))
-        arrival = PASSED_ON.get(m % 20)
+        arrival = PLACE.get(m % 20)
         arrival = 20 if arrival is None else arrival + (2 if arrival > 20 else 10) * (m // 20)
         return pltpu.make_async_remote_copy(
             src_ref=ref,
@@ -95,23 +157,8 @@
         ref = self.buf.at[pl.ds(0, count)]
         pltpu.make_async_copy(ref, ref, sem).wait()
 
-    def stage(self, s):
-        with jax.named_scope(f"g{self.number}s{s}"):
-            if s == 4:
-                self.whole(4, self.recv.at[self.number, 20])
-                return
-            then = [
-                [(None, (0, 1, 2, 3))],
-                [(0, (4, 6, 7)), (1, (5, 8, 9)), (2, (10,)), (3, (11,))],
-                [(4, ()), (5, (12, 13)), (6, (14,)), (7, (15,)), (8, (16,)), (9, (17,))],
-                [(12, (18,)), (13, (19,))],
-            ][s]
-            for wait, starts in then:
-                for turn in (0, 20):
-                    if wait is not None:
-                        self.copy(turn + wait).wait_recv()
-                    for m in starts:
-                        self.copy(turn + m).start()
+    def leaves(self):
+        self.whole(4, self.recv.at[self.number, 20])
 
     def finish(self):
         for stage, count in enumerate((4, 6, 4, 1)):
@@ -179,41 +226,43 @@
     named = [(routes_ref[k : k + 1, :] == expert).astype(F32) for k in (0, 1)]
     earlier = (iota((128, 128), 0) < iota((128, 128), 1)).astype(BF16)
     before = dot((named[0] + named[1]).astype(BF16), earlier)
-    slot = iota((512, 128), 0)
-    took = []
+    target = []
     for k in (0, 1):
         rank = jnp.sum(named[k] * before, axis=0, keepdims=True).astype(jnp.int32)
-        took.append((routes_ref[k : k + 1, :] * CAP + rank == slot).astype(F32))
+        route = routes_ref[k : k + 1, :]
+        away = (z + 16 - (route >> 1)) & 15
+        turn = jnp.zeros_like(route)
+        for i, dz in enumerate(REACH):
+            turn = jnp.where(away == dz % 16, i, turn)
+        target.append((turn * 2 + ((route + core) & 1)) * CAP + rank)
     own = normed[:, pl.ds(pl.multiple_of(tp * 128, 128), 128)]
-    outgoing[...] = dot((took[0] + took[1]).astype(BF16), own).astype(BF16)
-
+
+    def took(c):
+        slot = iota((CHUNK, 128), 0) + c * CHUNK
+        return [(target[k] == slot).astype(F32) for k in (0, 1)]
+
+    def pack(c):
+        first, second = took(c)
+        outgoing[c * CHUNK : (c + 1) * CHUNK] = dot((first + second).astype(BF16), own).astype(BF16)
+
+    pack(0)
     with jax.named_scope("enter"):
         pl.semaphore_wait(barrier, len(SLOTS) - 1 + 4)
 
-    def block_of(k):
-        return pl.ds((k % 8) * CAP, CAP)
-
-    def row_send(k):
-        dz, flip = SLOTS[k]
-        there = SLOT_OF[(-dz % 16, flip)]
-        expert = far(dz, flip)
-        return pltpu.make_async_remote_copy(
-            src_ref=outgoing.at[pl.ds(pl.multiple_of(expert * CAP, CAP), CAP)],
-            dst_ref=rows_buf.at[there // 8, tp, block_of(there)],
-            send_sem=z_send,
-            recv_sem=z_recv.at[there // 8],
-            device_id=(expert, tp),
-            device_id_type=MESH,
-        )
-
     def send_chunk(c):
-        for k in range(1, 32):
+        for k in range(max(1, 8 * c), 8 * c + 8):
             dz, flip = SLOTS[k]
-            if SLOT_OF[(-dz % 16, flip)] // 8 == c:
-                row_send(k).start()
+            pltpu.make_async_remote_copy(
+                src_ref=outgoing.at[pl.ds(k * CAP, CAP)],
+                dst_ref=rows_buf.at[c, tp, pl.ds((k - 8 * c) * CAP, CAP)],
+                send_sem=z_send,
+                recv_sem=z_recv.at[c],
+                device_id=(far(-dz, flip), tp),
+                device_id_type=MESH,
+            ).start()
 
     send_chunk(0)
-    rows_buf[0, tp, 0:CAP] = outgoing[pl.ds(pl.multiple_of(ep * CAP, CAP), CAP)]
+    rows_buf[0, tp, 0:CAP] = outgoing[0:CAP]
 
     def rows_arrived(c):
         if c == 0:
@@ -390,16 +439,15 @@
         if c == 0:
             loads[4].wait()
         res[c * CHUNK : (c + 1) * CHUNK] = dot(joined(hid_buf.at[c]), wd[...]).astype(BF16)
-        home = pl.ds(pl.multiple_of(ep * CAP, CAP), CAP)
         for k in range(8 * c, 8 * c + 8):
             if k == 0:
-                returned[home] = res[0:CAP]
+                returned[0:CAP] = res[0:CAP]
                 continue
             pltpu.make_async_remote_copy(
                 src_ref=res.at[pl.ds(k * CAP, CAP)],
-                dst_ref=returned.at[home],
+                dst_ref=returned.at[pl.ds(k * CAP, CAP)],
                 send_sem=r_send,
-                recv_sem=r_recv,
+                recv_sem=r_recv.at[c],
                 device_id=(far(*SLOTS[k]), tp),
                 device_id_type=MESH,
             ).start()
@@ -418,90 +466,81 @@
             total += dot(both_rows, jnp.concatenate([w, w], axis=0))
         return total
 
-    def arrive(c):
-        with jax.named_scope(f"arrive{c}"):
-            rows_arrived(c)
-        rows[c].stage(0)
-
-    def up(c):
-        rows[c].stage(4)
-        with jax.named_scope(f"up{c}"):
-            up_part(c)
-        hid[c].stage(0)
-
-    def down(c):
-        with jax.named_scope(f"down{c}"):
-            down_part(c)
-
-    with jax.named_scope("shared_part"):
-        shared_part()
-    arrive(0)
-    for c in (1, 2, 3):
-        send_chunk(c)
-    shared.stage(0)
-    with jax.named_scope("scan"):
-        scan_part()
-    rows[0].stage(1)
-    shared.stage(1)
-    loads[14].wait()
-    weighted = jnp.transpose(took[0] * rw_ref[0:1, :] + took[1] * rw_ref[1:2, :])
-    rounded = weighted.astype(BF16)
-    back_hi[...] = rounded
-    back_lo[...] = (weighted - rounded.astype(F32)).astype(BF16)
-    with jax.named_scope("pair"):
-        pair_part()
-    rows[0].stage(2)
-    shared.stage(2)
-    arrive(1)
-    rows[0].stage(3)
-    shared.stage(3)
-    arrive(2)
-    rows[1].stage(1)
-    up(0)
-    shared.stage(4)
-    arrive(3)
-    rows[2].stage(1)
-    rows[1].stage(2)
-    hid[0].stage(1)
-    with jax.named_scope("mixer_part"):
-        mixer_part()
-    mixed.stage(0)
-    rows[3].stage(1)
-    rows[2].stage(2)
-    rows[1].stage(3)
-    hid[0].stage(2)
-    mixed.stage(1)
-    up(1)
-    rows[2].stage(3)
-    rows[3].stage(2)
-    hid[0].stage(3)
-    mixed.stage(2)
-    up(2)
-    rows[3].stage(3)
-    hid[1].stage(1)
-    hid[0].stage(4)
-    mixed.stage(3)
-    up(3)
-    hid[1].stage(2)
-    hid[2].stage(1)
-    down(0)
-    mixed.stage(4)
-    hid[1].stage(3)
-    hid[2].stage(2)
-    hid[3].stage(1)
+    def back_part():
+        loads[14].wait()
+        for c in range(CHUNKS):
+            first, second = took(c)
+            weighted = jnp.transpose(first * rw_ref[0:1, :] + second * rw_ref[1:2, :])
+            rounded = weighted.astype(BF16)
+            columns = slice(c * CHUNK, (c + 1) * CHUNK)
+            back_hi[:, columns] = rounded
+            back_lo[:, columns] = (weighted - rounded.astype(F32)).astype(BF16)
+
+    def gain_part(c):
+        with jax.named_scope(f"back{c}"):
+            some = slice(CAP if c == 0 else c * CHUNK, (c + 1) * CHUNK)
+            came = returned.at[some]
+            pltpu.make_async_copy(came, came, r_recv.at[c]).wait()
+        some = slice(c * CHUNK, (c + 1) * CHUNK)
+        block = returned[some]
+        return dot(back_hi[:, some], block) + dot(back_lo[:, some], block)
+
+    gathers = {("shared", 0): shared, ("mixed", 0): mixed}
+    for c in range(CHUNKS):
+        gathers["rows", c], gathers["hid", c] = rows[c], hid[c]
+
+    def begin(gather):
+        for m in range(4):
+            for turn in (0, 20):
+                gather.copy(turn + m).start()
+
+    shared_part()
+    for event in schedule():
+        name, which = event[:2]
+        if name == "message":
+            _, gather, turn, m = event
+            gathers[gather].copy(20 * turn + m).wait_recv()
+            for following in THEN[m]:
+                gathers[gather].copy(20 * turn + following).start()
+        elif name == "leaves":
+            gathers[which].leaves()
+        elif name == "arrive":
+            with jax.named_scope(f"arrive{which}"):
+                rows_arrived(which)
+            begin(rows[which])
+            if which == 0:
+                for c in (1, 2, 3):
+                    pack(c)
+                    send_chunk(c)
+        elif name == "shared":
+            begin(shared)
+        elif name == "scan":
+            with jax.named_scope("scan"):
+                scan_part()
+        elif name == "pair":
+            pair_part()
+        elif name == "back":
+            with jax.named_scope("back"):
+                back_part()
+        elif name == "mixer":
+            with jax.named_scope("mixer_part"):
+                mixer_part()
+            begin(mixed)
+        elif name == "up":
+            with jax.named_scope(f"up{which}"):
+                up_part(which)
+            begin(hid[which])
+        elif name == "down":
+            with jax.named_scope(f"down{which}"):
+                down_part(which)
+        elif name == "mix_out":
+            with jax.named_scope("mix_out"):
+                loads[6].wait()
+                mix_ref[...] = spread_out(mix_buf, mixw).astype(BF16)
     loads[5].wait()
-    loads[6].wait()
-    mix_ref[...] = spread_out(mix_buf, mixw).astype(BF16)
-    hid[1].stage(4)
-    hid[2].stage(3)
-    hid[3].stage(2)
-    down(1)
-    hid[2].stage(4)
-    hid[3].stage(3)
-    down(2)
     common = spread_out(sh_buf, sd)
-    hid[3].stage(4)
-    down(3)
+    for c in range(CHUNKS - 1):
+        common += gain_part(c)
 
     with jax.named_scope("finish"):
         for gather in rows + hid + [mixed, shared]:
@@ -517,9 +556,7 @@
     pltpu.make_async_copy(sent, sent, z_send).wait()
     back = returned.at[pl.ds(0, 31 * CAP)]
     pltpu.make_async_copy(back, back, r_send).wait()
-    with jax.named_scope("last"):
-        pltpu.make_async_copy(back, back, r_recv).wait()
-    common += dot(back_hi[...], returned[...]) + dot(back_lo[...], returned[...])
+    common += gain_part(CHUNKS - 1)
     exp_ref[...] = common.astype(BF16)
 
 
@@ -580,7 +617,7 @@
             DMA((16,)),
             DMA((16,)),
             DMA,
-            DMA,
+            DMA((CHUNKS,)),
         ],
         compiler_params=pltpu.CompilerParams(
             collective_id=0, has_side_effects=True, vmem_limit_bytes=67_043_328

time: 87.8 us -> 82.4 us (0.938)
  Pallas kernels: 84.9 us -> 79.5 us
    pallas_call x1, Pallas kernels: 84.9 us -> 79.5 us  [shards(): pl.pallas_call(body, out_shape=(jax.ShapeDtypeStruct((256, 128), BF16), j...]
where the time goes in v3:
time: 82.4 us; the launch traced here: 82.3 us
  Pallas kernels  79.5 us (96%)
  local copies, waits for them, and re-layouts  2.1 us (3%)
    pallas_call x1, Pallas kernels, shards(): pl.pallas_call(body, out_shape=(jax.ShapeDtypeStruct((256, 128), BF16), j...  79.5 us
    unnamed x4, local copies, waits for them, and re-layouts  2.1 us

profile of v3, /device:TPU:1, one launch (start us, length us, event | category | flops | bytes accessed | tf_op | source)
XLA Modules:
  0.0 82.3 jit_solution(205025478814797948)
XLA Ops:
  0.6 79.5 %shard_map.167 = (bf16[256,128]{1,0:T(8,128)(2,1)}, bf16[128,128]{1,0:T(8,128)(2,1)}) custom-call(f32[4]{0:T(128)} %step_ref.1, bf16[64,256]{1,0:T(8,128)(2,1)} %bitcast.20, f32[4,256]{1,0:T(4,128)} %bitcast.23, bf16[128,64]{1,0:T(8,128)(2,1)} %bitcast.21, f32[128,64]{1,0:T(8,128)} %bitcast.19, bf16[128,2048]{1,0:T(8,128)(2,1)} %e_hbm.1, ...), custom_call_target="tpu_custom_call" | custom-call | tf_op jit(solution)/shard_map/pallas_call | solution.py:571
  80.2 0.0 copy-start
  80.2 1.5 %copy.20 = bf16[256,128]{1,0:T(8,128)(2,1)} copy(bf16[256,128]{1,0:T(8,128)(2,1)} %get-tuple-element.4) | data formatting | bytes 131072
  81.7 0.0 copy-done
  81.7 0.6 copy.21
Async XLA Ops:
  80.2 1.5 %copy-start = (bf16[128,128]{1,0:T(8,128)(2,1)S(1)}, bf16[128,128]{1,0:T(8,128)(2,1)}, u32[]{:S(2)}) copy-start(bf16[128,128]{1,0:T(8,128)(2,1)} %get-tuple-element.5) | copy-start | bytes 98308

commit v4 on v3

--- a/solution.py
+++ b/solution.py
@@ -48,7 +48,7 @@
     return jnp.concatenate([ref[0, at, :], ref[1, at, :]], axis=1)
 
 
-THEN = {0: (4, 6, 7), 1: (5, 8, 9), 2: (10,), 3: (11,), 4: (), 5: (12, 13)}
+THEN = {0: (4, 6, 7), 1: (5, 8, 9), 2: (10,), 3: (11,), 4: (12, 13), 5: (12, 13)}
 THEN = {**THEN, 6: (14,), 7: (15,), 8: (16,), 9: (17,), 12: (18,), 13: (19,)}
 PLACE = {**{m: m for m in range(10)}, 12: 21, 13: 22}
 WHOLE = (0, 1, 2, 3, 6, 7, 8, 9, 12, 13)
@@ -56,30 +56,45 @@
 BACKWARD = [0, 1] * 10
 
 
-def schedule(hop=1.9, rate=46600.0, later=(0.0, 7.0, 7.0, 7.0), mixer_at=14.0):
+def passed_on(here, gather, turn, m):
+    here.add((gather, turn, m))
+    if m in (4, 5) and (gather, turn, 9 - m) not in here:
+        return ()
+    return THEN[m]
+
+
+def schedule(hop=2.3, rate=43000.0, later=(0.0, 7.0, 7.0, 14.0), mixer_at=28.0, trace=None):
     size = {("shared", 0): 16384, ("mixed", 0): 32768}
-    rank = {("shared", 0): 0.5, ("mixed", 0): 1.5}
+    rank = {("shared", 0): 0.5, ("mixed", 0): 3.5}
     for c in range(CHUNKS):
-        size["rows", c], size["hid", c] = 32768, 65536
-        rank["rows", c] = rank["hid", c] = c
-    cost = {"scan": 2.2, "pair": 0.1, "back": 0.5, "mixer": 1.9, "mix_out": 0.6, "up": 0.47, "down": 0.47}
-    urgency = {"up": 1, "down": 2, "scan": 3, "pair": 3, "back": 4, "mixer": 3, "mix_out": 4}
-    now, free = 0.0, [0.0] * 4
+        size["rows", c] = 32768
+        rank["rows", c] = c
+    cost = {"scan": 2.2, "pair": 0.1, "back": 0.3, "mixer": 1.9, "mix_out": 0.6, "up": 0.47, "down": 0.35, "sum": 0.1}
+    urgency = {"up": 1, "down": 1, "scan": 3, "pair": 3, "back": 4, "mixer": 3, "mix_out": 4, "sum": 0}
+    now, free = 0.0, [0.5] * 4
     coming, ready, events = [], [], []
     ends = {gather: [] for gather in size}
     seen = {gather: 0 for gather in size}
-
-    def send(gather, turn, m):
+    count, here = {}, set()
+
+    def use(link, amount):
         nonlocal now
         now += 0.007
+        free[link] = max(now, free[link]) + amount / rate
+        return free[link] + hop
+
+    def later_on(at, order, event):
+        heapq.heappush(coming, (at, order, event))
+
+    def send(gather, turn, m):
         link = (RING[m] ^ turn) * 2 + BACKWARD[m]
-        free[link] = max(now, free[link]) + size[gather] / (2 if m in WHOLE else 4) / rate
+        at = use(link, size[gather] / (2 if m in WHOLE else 4))
         if m in THEN:
-            heapq.heappush(coming, (free[link] + hop, rank[gather], ("message", gather, turn, m)))
+            later_on(at, rank[gather], ("message", gather, turn, m))
             return
-        ends[gather].append(free[link] + hop)
+        ends[gather].append(at)
         if len(ends[gather]) == 16:
-            heapq.heappush(coming, (max(ends[gather]), rank[gather], ("leaves", gather)))
+            later_on(max(ends[gather]), rank[gather], ("leaves", gather))
 
     def begin(gather):
         for m in range(4):
@@ -87,9 +102,11 @@
                 send(gather, turn, m)
 
     for c in range(CHUNKS):
-        heapq.heappush(coming, (later[c], 0.0, ("arrive", c)))
+        later_on(later[c], 0.0, ("arrive", c))
     for at, name in ((0.0, "shared"), (0.0, "scan"), (4.5, "pair"), (5.0, "back"), (mixer_at, "mixer")):
-        heapq.heappush(coming, (at, 1.5, (name, 0)))
+        later_on(at, 1.5, (name, 0))
+    for at, event in ((0.02, ("relay", 0)), (1.0, ("relay", 1)), (1.5, ("weights", 2)), (4.5, ("weights", 3))):
+        later_on(at, 9.0, event)
     while coming or ready:
         while coming and (coming[0][0] <= now or not ready):
             at, order, event = heapq.heappop(coming)
@@ -97,17 +114,42 @@
             heapq.heappush(ready, (urgency.get(event[0], 0), order, at, event))
         event = heapq.heappop(ready)[3]
         events.append(event)
+        if trace is not None:
+            trace[event] = now
         now += cost.get(event[0], 0.01)
         name, which = event[:2]
-        if name in ("arrive", "shared", "mixer", "up"):
-            begin(({"arrive": "rows", "up": "hid", "mixer": "mixed"}.get(name, name), which))
-        if name in ("message", "leaves"):
+        if name in ("arrive", "shared", "mixer"):
+            begin(({"arrive": "rows", "mixer": "mixed"}.get(name, name), which))
+        elif name == "weights":
+            for link in range(4):
+                use(link, 65536)
+            later_on(max(use(link, 32768) for link in range(4)), 9.0, ("relay", which))
+        elif name == "relay":
+            for link in range(4):
+                use(link, 32768)
+        elif name == "up":
+            for turn in (0, 1):
+                for side in (0, 1):
+                    later_on(use(2 * turn + side, 32768), which, ("near", which, turn, side))
+        elif name == "near":
+            turn, side = event[2:]
+            at = use(2 * turn + side, 16384)
+            count.setdefault((which, turn), []).append(at)
+            if len(count[which, turn]) == 2:
+                later_on(max(count[which, turn]), which, ("down", which, turn))
+        elif name == "down":
+            turn = 1 - event[2]
+            at = max(use(2 * turn + side, 16384) for side in (0, 0, 1))
+            count.setdefault(which, []).append(at)
+            if len(count[which]) == 2:
+                later_on(max(count[which]) + 0.5, which, ("sum", which))
+        elif name in ("message", "leaves"):
             if name == "message":
-                for m in THEN[event[3]]:
+                for m in passed_on(here, which, *event[2:]):
                     send(which, event[2], m)
             seen[which] += 1
             if seen[which] == 25:
-                last = {"rows": "up", "hid": "down", "mixed": "mix_out"}.get(which[0])
+                last = {"rows": "up", "mixed": "mix_out"}.get(which[0])
                 if last:
                     heapq.heappush(ready, (urgency[last], rank[which], now, (last, which[1])))
     return events
@@ -185,10 +227,10 @@
     step_ref, x_hbm, shift_hbm, imap_hbm, rout_hbm, e_hbm, gain_hbm, routes_hbm, rw_hbm,
     mixw_hbm, wg_hbm, wu_hbm, wd_hbm, sg_hbm, su_hbm, sd_hbm,
     mix_ref, exp_ref,
-    x_ref, shift_ref, imap_ref, rout_ref, e_ref, gain_ref, routes_ref, rw_ref, mixw, wg, wu, wd, sgu, sd,
-    normed, outgoing, back_hi, back_lo, rows_buf, hid_buf, res, returned, mix_buf, sh_buf, pair, chips,
+    x_ref, shift_ref, imap_ref, rout_ref, e_ref, gain_ref, routes_ref, rw_ref, mixw, wg, wu, wd, wd_of, relay, sgu, sd,
+    normed, outgoing, back_hi, back_lo, rows_buf, hid_buf, part, parts, res, returned, mix_buf, sh_buf, pair, chips,
     push_r, push_i, mag, ph_r, ph_i, keep,
-    load_sem, g_send, g_recv, z_send, z_recv, s_send, s_recv, r_send, r_recv,
+    load_sem, g_send, g_recv, h_send, h_recv, w_send, w_recv, relay_recv, z_send, z_recv, s_send, s_recv, r_send, r_recv,
 ):
     ep, tp = lax.axis_index("ep"), lax.axis_index("tp")
     z, core = ep // 2, ep % 2
@@ -213,7 +255,7 @@
     barrier = pltpu.get_barrier_semaphore()
     for dz, flip in SLOTS[1:]:
         pl.semaphore_signal(barrier, inc=1, device_id=(far(dz, flip), tp), device_id_type=MESH)
-    for ny, nx in ((y, (x + 1) % 4), (y, (x + 3) % 4), ((y + 1) % 4, x), ((y + 3) % 4, x)):
+    for ny, nx in [(y, (x + d) % 4) for d in (1, 2, 3)] + [((y + d) % 4, x) for d in (1, 2, 3)]:
         pl.semaphore_signal(barrier, inc=1, device_id=(ep, ny * 4 + nx), device_id_type=MESH)
 
     with jax.named_scope("load"):
@@ -247,7 +289,7 @@
 
     pack(0)
     with jax.named_scope("enter"):
-        pl.semaphore_wait(barrier, len(SLOTS) - 1 + 4)
+        pl.semaphore_wait(barrier, len(SLOTS) - 1 + 6)
 
     def send_chunk(c):
         for k in range(max(1, 8 * c), 8 * c + 8):
@@ -371,9 +413,8 @@
 
     place = (ep, y, x)
     rows = [Gather(rows_buf.at[c], g_send, g_recv, c, place) for c in range(CHUNKS)]
-    hid = [Gather(hid_buf.at[c], g_send, g_recv, CHUNKS + c, place) for c in range(CHUNKS)]
-    mixed = Gather(mix_buf, g_send, g_recv, 2 * CHUNKS, place)
-    shared = Gather(sh_buf, g_send, g_recv, 2 * CHUNKS + 1, place)
+    mixed = Gather(mix_buf, g_send, g_recv, CHUNKS, place)
+    shared = Gather(sh_buf, g_send, g_recv, CHUNKS + 1, place)
 
     def packed(top, bottom):
         first = (iota((64, 128), 1) == iota((64, 128), 0)).astype(BF16)
@@ -433,12 +474,110 @@
             loads[2].wait()
             loads[3].wait()
         piece = joined(rows_buf.at[c])
-        hid_buf[c, tp] = (silu(dot(piece, wg[...])) * dot(piece, wu[...])).astype(BF16)
-
-    def down_part(c):
-        if c == 0:
-            loads[4].wait()
-        res[c * CHUNK : (c + 1) * CHUNK] = dot(joined(hid_buf.at[c]), wd[...]).astype(BF16)
+        hidden = (silu(dot(piece, wg[...])) * dot(piece, wu[...])).astype(BF16)
+        hid_buf[c, 0, x] = hidden[: CHUNK // 2]
+        hid_buf[c, 1, y] = hidden[CHUNK // 2 :]
+        for turn in (0, 1):
+            for side in (0, 1):
+                hidden_copy(c, turn, side).start()
+
+    def along(turn, d):
+        return (ep, ((y + d) % 4) * 4 + x) if turn else (ep, y * 4 + (x + d) % 4)
+
+    def hidden_copy(c, turn, side, passed=False):
+        mine = y if turn else x
+        back = 3 if side == 0 else 1
+        ref = hid_buf.at[c, turn, (mine + back) % 4 if passed else mine]
+        if passed:
+            ref = ref.at[pl.ds(side * (CHUNK // 4), CHUNK // 4)]
+        return pltpu.make_async_remote_copy(
+            src_ref=ref,
+            dst_ref=ref,
+            send_sem=h_send.at[c, turn, 0],
+            recv_sem=h_recv.at[c, turn, 2 if passed else side],
+            device_id=along(turn, 1 if side == 0 else 3),
+            device_id_type=MESH,
+        )
+
+    def weight_copy(turn, d, j):
+        source = wd.at[j, (x + d) % 4] if turn else wd.at[(y + d) % 4, j]
+        if d == 0:
+            return pltpu.make_async_copy(source, wd_of.at[turn, 0, j], w_recv.at[turn, 0])
+        return pltpu.make_async_remote_copy(
+            src_ref=source,
+            dst_ref=wd_of.at[turn, 4 - d, j],
+            send_sem=w_send.at[turn, d],
+            recv_sem=w_recv.at[turn, 4 - d],
+            device_id=along(1 - turn, d),
+            device_id_type=MESH,
+        )
+
+    def relay_copy(turn, side, j, passed):
+        rows_here = pl.ds(side * 128, 128)
+        source = wd.at[j, (x + 2) % 4, rows_here] if turn else wd.at[(y + 2) % 4, j, rows_here]
+        hold = relay.at[turn, side, j]
+        return pltpu.make_async_remote_copy(
+            src_ref=hold if passed else source,
+            dst_ref=wd_of.at[turn, 2, j, rows_here] if passed else hold,
+            send_sem=w_send.at[turn, 0 if passed else 2],
+            recv_sem=w_recv.at[turn, 2] if passed else relay_recv.at[turn, side, j],
+            device_id=along(1 - turn, 3 if side else 1),
+            device_id_type=MESH,
+        )
+
+    def send_weights(j):
+        for turn in (0, 1):
+            for d in (1, 3):
+                weight_copy(turn, d, j).start()
+        for turn in (0, 1):
+            for side in (0, 1):
+                relay_copy(turn, side, j, False).start()
+            weight_copy(turn, 0, j).start()
+
+    def relay_weights(j):
+        for turn in (0, 1):
+            for side in (0, 1):
+                relay_copy(turn, side, j, False).wait_recv()
+                relay_copy(turn, side, j, True).start()
+
+    def wait_weights():
+        for turn in (0, 1):
+            for d in range(4):
+                ref = wd_of.at[turn, d]
+                pltpu.make_async_copy(ref, ref, w_recv.at[turn, d]).wait()
+
+    def part_copy(c, turn, d):
+        return pltpu.make_async_remote_copy(
+            src_ref=part.at[c, turn, d],
+            dst_ref=parts.at[c, turn, d],
+            send_sem=h_send.at[c, turn, 1],
+            recv_sem=h_recv.at[c, turn, 3],
+            device_id=along(1 - turn, d),
+            device_id_type=MESH,
+        )
+
+    def down_part(c, turn):
+        ref = hid_buf.at[c, turn, 0]
+        pltpu.make_async_copy(ref, ref, h_recv.at[c, turn, 2]).wait()
+        hidden = jnp.concatenate([hid_buf[c, turn, i] for i in range(4)], axis=1)
+        for pairs in ((1, 3), (2, 0)):
+            weight = jnp.concatenate([wd_of[turn, d].reshape(1024, 128) for d in pairs], axis=1)
+            sums = dot(hidden, weight).astype(BF16)
+            for n, d in enumerate(pairs):
+                value = sums[:, n * 128 : (n + 1) * 128]
+                if d == 0:
+                    parts[c, turn, 0] = value
+                else:
+                    part[c, turn, d] = value
+                    part_copy(c, turn, d).start()
+
+    def sum_part(c):
+        for turn in (0, 1):
+            ref = parts.at[c, turn, pl.ds(1, 3)]
+            pltpu.make_async_copy(ref, ref, h_recv.at[c, turn, 3]).wait()
+            total = sum(parts[c, turn, d].astype(F32) for d in range(4))
+            start = c * CHUNK + turn * (CHUNK // 2)
+            res[start : start + CHUNK // 2] = total.astype(BF16)
         for k in range(8 * c, 8 * c + 8):
             if k == 0:
                 returned[0:CAP] = res[0:CAP]
@@ -487,20 +626,26 @@
 
     gathers = {("shared", 0): shared, ("mixed", 0): mixed}
     for c in range(CHUNKS):
-        gathers["rows", c], gathers["hid", c] = rows[c], hid[c]
+        gathers["rows", c] = rows[c]
 
     def begin(gather):
         for m in range(4):
             for turn in (0, 20):
                 gather.copy(turn + m).start()
 
+    loads[4].wait()
+    send_weights(0)
+    send_weights(1)
     shared_part()
+    for c in (1, 2, 3):
+        pack(c)
+    down_first, here = True, set()
     for event in schedule():
         name, which = event[:2]
         if name == "message":
             _, gather, turn, m = event
             gathers[gather].copy(20 * turn + m).wait_recv()
-            for following in THEN[m]:
+            for following in passed_on(here, gather, turn, m):
                 gathers[gather].copy(20 * turn + following).start()
         elif name == "leaves":
             gathers[which].leaves()
@@ -510,7 +655,6 @@
             begin(rows[which])
             if which == 0:
                 for c in (1, 2, 3):
-                    pack(c)
                     send_chunk(c)
         elif name == "shared":
             begin(shared)
@@ -526,13 +670,28 @@
             with jax.named_scope("mixer_part"):
                 mixer_part()
             begin(mixed)
+        elif name == "weights":
+            send_weights(which)
+        elif name == "relay":
+            with jax.named_scope(f"relay{which}"):
+                relay_weights(which)
         elif name == "up":
             with jax.named_scope(f"up{which}"):
                 up_part(which)
-            begin(hid[which])
+        elif name == "near":
+            with jax.named_scope(f"near{which}"):
+                hidden_copy(*event[1:]).wait_recv()
+                hidden_copy(*event[1:], passed=True).start()
         elif name == "down":
+            if down_first:
+                down_first = False
+                with jax.named_scope("weights"):
+                    wait_weights()
             with jax.named_scope(f"down{which}"):
-                down_part(which)
+                down_part(which, event[2])
+        elif name == "sum":
+            with jax.named_scope(f"sum{which}"):
+                sum_part(which)
         elif name == "mix_out":
             with jax.named_scope("mix_out"):
                 loads[6].wait()
@@ -543,8 +702,17 @@
         common += gain_part(c)
 
     with jax.named_scope("finish"):
-        for gather in rows + hid + [mixed, shared]:
+        for gather in rows + [mixed, shared]:
             gather.finish()
+        for turn in (0, 1):
+            for c in range(CHUNKS):
+                ref = hid_buf.at[c, turn, pl.ds(0, 3)]
+                pltpu.make_async_copy(ref, ref, h_send.at[c, turn, 0]).wait()
+                ref = part.at[c, turn, pl.ds(1, 3)]
+                pltpu.make_async_copy(ref, ref, h_send.at[c, turn, 1]).wait()
+            for d in range(4):
+                ref = wd_of.at[turn, d]
+                pltpu.make_async_copy(ref, ref, w_send.at[turn, d]).wait()
         to_partner().wait_send()
         for dz in range(1, 16):
 
@@ -588,7 +756,9 @@
             V((1024, 128), BF16),
             V((2048, 256), BF16),
             V((2048, 256), BF16),
-            V((4096, 128), BF16),
+            V((4, 4, 256, 128), BF16),
+            V((2, 4, 4, 256, 128), BF16),
+            V((2, 2, 4, 128, 128), BF16),
             V((128, 2048), BF16),
             V((1024, 128), BF16),
             V((128, 2048), BF16),
@@ -596,7 +766,9 @@
             V((128, 512), BF16),
             V((128, 512), BF16),
             V((CHUNKS, 16, CHUNK, 128), BF16),
-            V((CHUNKS, 16, CHUNK, 256), BF16),
+            V((CHUNKS, 2, 4, CHUNK // 2, 256), BF16),
+            V((CHUNKS, 2, 4, CHUNK // 2, 128), BF16),
+            V((CHUNKS, 2, 4, CHUNK // 2, 128), BF16),
             V((512, 128), BF16),
             V((512, 128), BF16),
             V((16, 128, 128), BF16),
@@ -610,8 +782,13 @@
             V((32, 256), F32),
             V((4, 8, 256), F32),
             DMA((15,)),
-            DMA((2 * CHUNKS + 2, 4)),
-            DMA((2 * CHUNKS + 2, 25)),
+            DMA((CHUNKS + 2, 4)),
+            DMA((CHUNKS + 2, 25)),
+            DMA((CHUNKS, 2, 2)),
+            DMA((CHUNKS, 2, 4)),
+            DMA((2, 4)),
+            DMA((2, 4)),
+            DMA((2, 2, 4)),
             DMA,
             DMA((CHUNKS,)),
             DMA((16,)),
@@ -635,7 +812,7 @@
         mixer_weight,
         expert_switch_matrix[0],
         up_weight[0],
-        down_weight[0],
+        down_weight.reshape(4, 4, 256, 128),
         shared_gate.T,
         shared_up.T,
         shared_down,

time: 82.4 us -> 75 us (0.910)
  Pallas kernels: 79.5 us -> 72.1 us
    pallas_call x1, Pallas kernels: 79.5 us -> 72.1 us  [shards(): pl.pallas_call(body, out_shape=(jax.ShapeDtypeStruct((256, 128), BF16), j...]
where the time goes in v4:
time: 75 us; the launch traced here: 74.8 us
  Pallas kernels  72.1 us (96%)
  local copies, waits for them, and re-layouts  2.1 us (3%)
    pallas_call x1, Pallas kernels, shards(): pl.pallas_call(body, out_shape=(jax.ShapeDtypeStruct((256, 128), BF16), j...  72.1 us
    unnamed x4, local copies, waits for them, and re-layouts  2.1 us

profile of v4, /device:TPU:1, one launch (start us, length us, event | category | flops | bytes accessed | tf_op | source)
XLA Modules:
  0.0 74.8 jit_solution(6941557899276526335)
XLA Ops:
  0.6 72.1 %shard_map.167 = (bf16[256,128]{1,0:T(8,128)(2,1)}, bf16[128,128]{1,0:T(8,128)(2,1)}) custom-call(f32[4]{0:T(128)} %step_ref.1, bf16[64,256]{1,0:T(8,128)(2,1)} %bitcast.20, f32[4,256]{1,0:T(4,128)} %bitcast.23, bf16[128,64]{1,0:T(8,128)(2,1)} %bitcast.21, f32[128,64]{1,0:T(8,128)} %bitcast.19, bf16[128,2048]{1,0:T(8,128)(2,1)} %e_hbm.1, ...), custom_call_target="tpu_custom_call" | custom-call | tf_op jit(solution)/shard_map/pallas_call | solution.py:739
  72.7 0.0 copy-start
  72.7 1.5 %copy.20 = bf16[256,128]{1,0:T(8,128)(2,1)} copy(bf16[256,128]{1,0:T(8,128)(2,1)} %get-tuple-element.4) | data formatting | bytes 131072
  74.2 0.0 copy-done
  74.2 0.6 copy.21
Async XLA Ops:
  72.7 1.5 %copy-start = (bf16[128,128]{1,0:T(8,128)(2,1)S(1)}, bf16[128,128]{1,0:T(8,128)(2,1)}, u32[]{:S(2)}) copy-start(bf16[128,128]{1,0:T(8,128)(2,1)} %get-tuple-element.5) | copy-start | bytes 98308

commit v5 on v4

--- a/solution.py
+++ b/solution.py
@@ -63,7 +63,7 @@
     return THEN[m]
 
 
-def schedule(hop=2.3, rate=43000.0, later=(0.0, 7.0, 7.0, 14.0), mixer_at=28.0, trace=None):
+def schedule(hop=2.3, rate=43000.0, later=(0.0, 7.0, 7.0, 14.0), mixer_at=27.0, trace=None):
     size = {("shared", 0): 16384, ("mixed", 0): 32768}
     rank = {("shared", 0): 0.5, ("mixed", 0): 3.5}
     for c in range(CHUNKS):
@@ -75,7 +75,7 @@
     coming, ready, events = [], [], []
     ends = {gather: [] for gather in size}
     seen = {gather: 0 for gather in size}
-    count, here = {}, set()
+    count, here, straight = {}, set(), {}
 
     def use(link, amount):
         nonlocal now
@@ -105,7 +105,7 @@
         later_on(later[c], 0.0, ("arrive", c))
     for at, name in ((0.0, "shared"), (0.0, "scan"), (4.5, "pair"), (5.0, "back"), (mixer_at, "mixer")):
         later_on(at, 1.5, (name, 0))
-    for at, event in ((0.02, ("relay", 0)), (1.0, ("relay", 1)), (1.5, ("weights", 2)), (4.5, ("weights", 3))):
+    for at, event in ((0.015, ("weights", 2)), (2.4, ("relay", 0)), (2.4, ("relay", 1)), (3.0, ("weights", 3))):
         later_on(at, 9.0, event)
     while coming or ready:
         while coming and (coming[0][0] <= now or not ready):
@@ -131,9 +131,12 @@
             for turn in (0, 1):
                 for side in (0, 1):
                     later_on(use(2 * turn + side, 32768), which, ("near", which, turn, side))
+                if which == CHUNKS - 1:
+                    use(2 * turn, 32768)
+                    straight[turn] = use(2 * turn, 32768) + 0.8
         elif name == "near":
             turn, side = event[2:]
-            at = use(2 * turn + side, 16384)
+            at = straight[turn] if which == CHUNKS - 1 else use(2 * turn + side, 16384)
             count.setdefault((which, turn), []).append(at)
             if len(count[which, turn]) == 2:
                 later_on(max(count[which, turn]), which, ("down", which, turn))
@@ -231,10 +234,24 @@
     normed, outgoing, back_hi, back_lo, rows_buf, hid_buf, part, parts, res, returned, mix_buf, sh_buf, pair, chips,
     push_r, push_i, mag, ph_r, ph_i, keep,
     load_sem, g_send, g_recv, h_send, h_recv, w_send, w_recv, relay_recv, z_send, z_recv, s_send, s_recv, r_send, r_recv,
+    mix_val, exp_val, out_sem,
 ):
     ep, tp = lax.axis_index("ep"), lax.axis_index("tp")
     z, core = ep // 2, ep % 2
     y, x = tp // 4, tp % 4
+
+    def out_copy(k):
+        return pltpu.make_async_copy((mix_val, exp_val)[k], (mix_ref, exp_ref)[k], out_sem.at[k])
+
+    def far(dz, flip):
+        return ((z + dz + 16) % 16) * 2 + (core + flip) % 2
+
+    chips[...] = jnp.zeros_like(chips)
+    barrier = pltpu.get_barrier_semaphore()
+    for dz, flip in SLOTS[1:]:
+        pl.semaphore_signal(barrier, inc=1, device_id=(far(dz, flip), tp), device_id_type=MESH)
+    for ny, nx in [(y, (x + d) % 4) for d in (1, 2, 3)] + [((y + d) % 4, x) for d in (1, 2, 3)]:
+        pl.semaphore_signal(barrier, inc=1, device_id=(ep, ny * 4 + nx), device_id_type=MESH)
 
     loads = [
         pltpu.make_async_copy(src, dst, load_sem.at[k])
@@ -247,16 +264,6 @@
     ]
     for k in (7, 8, 9, 10, 11, 12, 13, 14, 0, 1, 2, 3, 4, 5, 6):
         loads[k].start()
-
-    def far(dz, flip):
-        return ((z + dz + 16) % 16) * 2 + (core + flip) % 2
-
-    chips[...] = jnp.zeros_like(chips)
-    barrier = pltpu.get_barrier_semaphore()
-    for dz, flip in SLOTS[1:]:
-        pl.semaphore_signal(barrier, inc=1, device_id=(far(dz, flip), tp), device_id_type=MESH)
-    for ny, nx in [(y, (x + d) % 4) for d in (1, 2, 3)] + [((y + d) % 4, x) for d in (1, 2, 3)]:
-        pl.semaphore_signal(barrier, inc=1, device_id=(ep, ny * 4 + nx), device_id_type=MESH)
 
     with jax.named_scope("load"):
         for k in (7, 8, 9):
@@ -480,6 +487,19 @@
         for turn in (0, 1):
             for side in (0, 1):
                 hidden_copy(c, turn, side).start()
+            if c == CHUNKS - 1:
+                straight_copy(c, turn).start()
+
+    def straight_copy(c, turn):
+        ref = hid_buf.at[c, turn, y if turn else x]
+        return pltpu.make_async_remote_copy(
+            src_ref=ref,
+            dst_ref=ref,
+            send_sem=h_send.at[c, turn, 0],
+            recv_sem=h_recv.at[c, turn, 2],
+            device_id=along(turn, 2),
+            device_id_type=MESH,
+        )
 
     def along(turn, d):
         return (ep, ((y + d) % 4) * 4 + x) if turn else (ep, y * 4 + (x + d) % 4)
@@ -681,7 +701,8 @@
         elif name == "near":
             with jax.named_scope(f"near{which}"):
                 hidden_copy(*event[1:]).wait_recv()
-                hidden_copy(*event[1:], passed=True).start()
+                if which < CHUNKS - 1:
+                    hidden_copy(*event[1:], passed=True).start()
         elif name == "down":
             if down_first:
                 down_first = False
@@ -695,7 +716,8 @@
         elif name == "mix_out":
             with jax.named_scope("mix_out"):
                 loads[6].wait()
-                mix_ref[...] = spread_out(mix_buf, mixw).astype(BF16)
+                mix_val[...] = spread_out(mix_buf, mixw).astype(BF16)
+                out_copy(0).start()
     loads[5].wait()
     common = spread_out(sh_buf, sd)
     for c in range(CHUNKS - 1):
@@ -725,7 +747,10 @@
     back = returned.at[pl.ds(0, 31 * CAP)]
     pltpu.make_async_copy(back, back, r_send).wait()
     common += gain_part(CHUNKS - 1)
-    exp_ref[...] = common.astype(BF16)
+    exp_val[...] = common.astype(BF16)
+    out_copy(1).start()
+    out_copy(0).wait()
+    out_copy(1).wait()
 
 
 def shards(
@@ -733,7 +758,6 @@
     norm_gain, routes, route_weight, expert_switch_matrix, up_weight, down_weight,
     shared_gate, shared_up, shared_down,
 ):
-    vmem = pl.BlockSpec(memory_space=pltpu.VMEM)
     hbm = pl.BlockSpec(memory_space=pltpu.HBM)
     V, DMA = pltpu.VMEM, pltpu.SemaphoreType.DMA
     return pl.pallas_call(
@@ -743,7 +767,7 @@
             jax.ShapeDtypeStruct((128, 128), BF16),
         ),
         in_specs=[pl.BlockSpec(memory_space=pltpu.SMEM)] + [hbm] * 15,
-        out_specs=(vmem, vmem),
+        out_specs=(hbm, hbm),
         scratch_shapes=[
             V((64, 256), BF16),
             V((4, 256), F32),
@@ -795,6 +819,9 @@
             DMA((16,)),
             DMA,
             DMA((CHUNKS,)),
+            V((256, 128), BF16),
+            V((128, 128), BF16),
+            DMA((2,)),
         ],
         compiler_params=pltpu.CompilerParams(
             collective_id=0, has_side_effects=True, vmem_limit_bytes=67_043_328

time: 75 us -> 74.1 us (0.988)
  Pallas kernels: 72.1 us -> 71.2 us
    pallas_call x1, Pallas kernels: 72.1 us -> 71.2 us  [shards(): pl.pallas_call(body, out_shape=(jax.ShapeDtypeStruct((256, 128), BF16), j...]
where the time goes in v5:
time: 74.1 us; the launch traced here: 73.9 us
  Pallas kernels  71.2 us (96%)
  local copies, waits for them, and re-layouts  2.1 us (3%)
    pallas_call x1, Pallas kernels, shards(): pl.pallas_call(body, out_shape=(jax.ShapeDtypeStruct((256, 128), BF16), j...  71.2 us
    unnamed x4, local copies, waits for them, and re-layouts  2.1 us

profile of v5, /device:TPU:1, one launch (start us, length us, event | category | flops | bytes accessed | tf_op | source)
XLA Modules:
  0.0 73.9 jit_solution(11168469128467221897)
XLA Ops:
  0.6 71.2 %shard_map.167 = (bf16[256,128]{1,0:T(8,128)(2,1)}, bf16[128,128]{1,0:T(8,128)(2,1)}) custom-call(f32[4]{0:T(128)} %step_ref.1, bf16[64,256]{1,0:T(8,128)(2,1)} %bitcast.20, f32[4,256]{1,0:T(4,128)} %bitcast.23, bf16[128,64]{1,0:T(8,128)(2,1)} %bitcast.21, f32[128,64]{1,0:T(8,128)} %bitcast.19, bf16[128,2048]{1,0:T(8,128)(2,1)} %e_hbm.1, ...), custom_call_target="tpu_custom_call" | custom-call | tf_op jit(solution)/shard_map/pallas_call | solution.py:763
  71.8 0.0 copy-start
  71.8 1.5 %copy.20 = bf16[256,128]{1,0:T(8,128)(2,1)} copy(bf16[256,128]{1,0:T(8,128)(2,1)} %get-tuple-element.4) | data formatting | bytes 131072
  73.3 0.0 copy-done
  73.3 0.6 copy.21
Async XLA Ops:
  71.8 1.5 %copy-start = (bf16[128,128]{1,0:T(8,128)(2,1)S(1)}, bf16[128,128]{1,0:T(8,128)(2,1)}, u32[]{:S(2)}) copy-start(bf16[128,128]{1,0:T(8,128)(2,1)} %get-tuple-element.5) | copy-start | bytes 98308
